TPU v7x, 256 devices: a whole 4x4x8 slice. The times are simulated.
256 devices in a mesh: ep: 16 (over y, x), tp: 16 (over z, core).
Axes of the slice: x: 4, y: 4, z: 8, core: 2. Of those that a mesh axis runs over, the one named last changes fastest.
Arguments:
- mixer_input_channels: bfloat16 [32768, 2048], P('ep', 'tp'), may hold values from -6 to 6
- output_gate_logits: bfloat16 [32768, 2048], P('ep', 'tp'), may hold values from -6 to 6
- head_group_input_map: bfloat16 [32768, 256], P('ep'), may hold values from -6 to 6
- head_group_output_map: bfloat16 [32768, 256], P('ep'), may hold values from -6 to 6
- input_channel_taps: bfloat16 [4, 2048], P(None, 'tp'), may hold values from -3 to 3
- input_map_taps: bfloat16 [4, 256], replicated, may hold values from -3 to 3
- output_map_taps: bfloat16 [4, 256], replicated, may hold values from -3 to 3
- step_logits: float32 [32, 32768], P('tp', 'ep'), may hold values from -5 to 5
- head_log_rate: float32 [32], P('tp'), may hold values from -20 to -2
- extra_log_decay: float32 [32, 32768], P('tp', 'ep'), may hold values from -1 to 0
- head_direct_scale: float32 [32], P('tp'), may hold values from 1 to 6
- gated_norm_scale: bfloat16 [2048], P('tp'), may hold values from 0.099609375 to 1.8984375
- mixer_output_weight: bfloat16 [2048, 2048], P('tp'), may hold values from -0.125 to 0.125
- second_batch_tokens: bfloat16 [4096, 2048], P('ep'), may hold values from -6 to 6
- pre_expert_norm_scale: bfloat16 [2048], replicated, may hold values from 0.099609375 to 1.8984375
- group_router_columns: bfloat16 [2048, 4], replicated
- expert_router_columns: bfloat16 [2048, 16], replicated
- routes: int32 [4096, 2], P('ep'), may hold values from 0 to 15, all different within a row; in each aligned block of 256 rows (0 to 255, 256 to 511, ...) at most 64 rows name the same one
- expert_gate_weight: bfloat16 [16, 2048, 4096], P('ep', None, 'tp'), may hold values from -0.125 to 0.125
- expert_up_weight: bfloat16 [16, 2048, 4096], P('ep', None, 'tp'), may hold values from -0.125 to 0.125
- expert_down_weight: bfloat16 [16, 4096, 2048], P('ep', 'tp'), may hold values from -0.125 to 0.125
Outputs:
- mixer_out: bfloat16 [32768, 2048], P(('ep', 'tp'))
- experts_out: bfloat16 [4096, 2048], P('ep', 'tp')
Inputs may be any that keep to these rules, and one draw needn't show every extreme that they name: `routes`: in each aligned block of 256 rows no expert is named more than 64 times, some expert exactly 64 times in some block; a row's two experts differ.
All inputs are finite; a program needn't handle non-finite values.
Results may differ from a plain program's by a relative error of at most 0.019.
Values may be sent and summed in bfloat16 or wider, within the bound.
A program may use at most 128 MiB of HBM per device.

v0:
```python
import jax
import jax.numpy as jnp
from jax import lax
from jax.sharding import PartitionSpec as P

HEADS = 32
STATE = 64
GROUPS = 4
BLOCK = 128


eps = 1e-06
exact_prec = lax.Precision.HIGHEST


def from_behind(value, axis, steps):
    count = lax.axis_size(axis)
    first, last = (max(0, -steps), min(count, count - steps))
    return lax.ppermute(value, axis, [(source, source + steps) for source in range(first, last)])


def from_everyone(value, axis):
    size = lax.axis_size(axis)
    return lax.all_to_all(
        jnp.broadcast_to(value[None], (size, *value.shape)), axis, 0, 0, tiled=True
    )


def gathered_once(value, axis):
    leaves = jax.tree.leaves(value)
    turns = sorted(range(len(leaves)), key=lambda k: -leaves[k].size)
    width = (1, *leaves[turns[0]].shape)[-1]
    lines = [
        jnp.pad(leaves[k].reshape(-1), (0, -leaves[k].size % width)).reshape(-1, width)
        for k in turns
    ]
    both, at, found = (from_everyone(jnp.concatenate(lines), axis), 0, {})
    for k, line in zip(turns, lines):
        slab = both[:, at : at + len(line)].reshape(len(both), -1)
        found[k] = slab[:, : leaves[k].size].reshape(-1, *leaves[k].shape)
        at += len(line)
    numbers = iter(range(len(leaves)))
    return jax.tree.map(lambda _: found[next(numbers)], value)


def folded_in_pairs(pieces, combine):
    while len(jax.tree.leaves(pieces)[0]) > 1:
        pieces = jax.vmap(combine)(
            *(jax.tree.map(lambda part: part[side::2], pieces) for side in (0, 1))
        )
    return jax.tree.map(lambda part: part[0], pieces)


def entering_2(value, axis, combine, identity):
    size, here = (lax.axis_size(axis), lax.axis_index(axis))
    passed = jnp.arange(size) < here

    def kept(part, zero, own):
        part = jnp.where(
            passed.reshape(-1, *(1 for _ in own.shape)),
            part.astype(own.dtype),
            jnp.asarray(zero, own.dtype),
        )
        return part

    pieces = gathered_once(
        jax.tree.map(lambda part, kind: part.astype(kind), value, (jnp.bfloat16, jnp.bfloat16)),
        axis,
    )
    return folded_in_pairs(jax.tree.map(kept, pieces, identity, value), combine)


def conv_with_rows(joined, before, taps):
    length = joined.shape[0]
    padded = jnp.concatenate([before, joined], axis=0).astype(jnp.float32)
    total = jnp.zeros(joined.shape, jnp.float32)
    for j in range(taps.shape[0]):
        total = total + taps[j].astype(jnp.float32) * padded[j : j + length]
    return jax.nn.silu(total).astype(jnp.bfloat16)


def chain_states(earlier, later):
    return (earlier[0] * later[1][:, None, None] + later[0], earlier[1] * later[1])


def slot_positions(route_rows, n_experts):
    flat = route_rows.reshape(-1)
    onehot = (flat[:, None] == jnp.arange(n_experts, dtype=jnp.int32)[None, :]).astype(jnp.int32)
    return jnp.sum(onehot * jnp.cumsum(onehot, axis=0), axis=1) - 1


def route_weights(group_logits, expert_logits, routes):
    n_groups = group_logits.shape[1]
    n_experts = expert_logits.shape[1]
    per_group = n_experts // n_groups
    group_lp = jax.nn.log_softmax(group_logits, axis=-1)
    inner_lp = jax.nn.log_softmax(expert_logits.reshape(-1, n_groups, per_group), axis=-1).reshape(
        -1, n_experts
    )
    total = jnp.repeat(group_lp, per_group, axis=1) + inner_lp
    pick = routes[:, :, None] == jnp.arange(n_experts, dtype=jnp.int32)[None, None, :]
    chosen = jnp.sum(jnp.where(pick, total[:, None, :], 0.0), axis=-1)
    return jax.nn.softmax(chosen, axis=-1)


def mixer_half(
    mixer_input_channels,
    output_gate_logits,
    head_group_input_map,
    head_group_output_map,
    input_channel_taps,
    input_map_taps,
    output_map_taps,
    step_logits,
    head_log_rate,
    extra_log_decay,
    head_direct_scale,
    gated_norm_scale,
    mixer_output_weight,
):
    length, width = mixer_input_channels.shape
    heads_dev = head_direct_scale.shape[0]
    head_dim = width // heads_dev
    group = lax.axis_index("tp") * heads_dev // (HEADS // GROUPS)
    first_col = group * STATE
    b_rows = lax.dynamic_slice_in_dim(head_group_input_map, first_col, STATE, 1)
    c_rows = lax.dynamic_slice_in_dim(head_group_output_map, first_col, STATE, 1)
    b_taps = lax.dynamic_slice_in_dim(input_map_taps, first_col, STATE, 1)
    c_taps = lax.dynamic_slice_in_dim(output_map_taps, first_col, STATE, 1)
    joined = jnp.concatenate([mixer_input_channels, b_rows, c_rows], axis=1)
    taps = jnp.concatenate([input_channel_taps, b_taps, c_taps], axis=1)
    reach = taps.shape[0] - 1
    before = from_behind(joined[length - reach :], "ep", 1)
    conv = conv_with_rows(joined, before, taps)
    nblk = length // BLOCK
    xs_f = conv[:, :width].astype(jnp.float32)
    bs_f = conv[:, width : width + STATE].astype(jnp.float32).reshape(nblk, BLOCK, STATE)
    cs_f = conv[:, width + STATE :].astype(jnp.float32).reshape(nblk, BLOCK, STATE)
    head_step_length = jax.nn.softplus(step_logits)
    position_log_decay = extra_log_decay - head_step_length * jnp.exp(head_log_rate)[:, None]
    cum = jnp.cumsum(position_log_decay.reshape(heads_dev, nblk, BLOCK), axis=2)
    step_blocks = jnp.transpose(head_step_length.reshape(heads_dev, nblk, BLOCK), (1, 2, 0))
    x_dt = xs_f.reshape(nblk, BLOCK, heads_dev, head_dim) * step_blocks[..., None]
    lower = jnp.tril(jnp.ones((BLOCK, BLOCK), bool))
    diff = cum[:, :, :, None] - cum[:, :, None, :]
    weight = jnp.where(lower, jnp.exp(jnp.where(lower, diff, 0.0)), 0.0)
    scores = jnp.einsum("bln,bsn->bls", cs_f, bs_f, precision=exact_prec)
    inner = jnp.einsum("bls,hbls,bshp->blhp", scores, weight, x_dt, precision=exact_prec)
    tail = jnp.exp(cum[:, :, -1:] - cum)
    block_state = jnp.einsum("bsn,hbs,bshp->bhpn", bs_f, tail, x_dt, precision=exact_prec)
    block_log = cum[:, :, -1]
    run_log = jnp.cumsum(block_log, axis=1)
    total_log = run_log[:, -1]
    own_state = jnp.einsum(
        "hb,bhpn->hpn", jnp.exp(total_log[:, None] - run_log), block_state, precision=exact_prec
    )
    own_decay = jnp.exp(total_log)
    entering, reached = entering_2(
        (own_state, own_decay),
        "ep",
        chain_states,
        (jnp.zeros_like(own_state), jnp.ones_like(own_decay)),
    )
    start_log = run_log - block_log
    earlier = jnp.arange(nblk)[:, None] > jnp.arange(nblk)[None, :]
    gap = start_log[:, :, None] - run_log[:, None, :]
    link = jnp.where(earlier, jnp.exp(jnp.where(earlier, gap, 0.0)), 0.0)
    prev = jnp.einsum("hbc,chpn->bhpn", link, block_state, precision=exact_prec)
    prev = prev + jnp.transpose(jnp.exp(start_log))[:, :, None, None] * entering[None]
    carried = jnp.einsum("bln,bhpn->blhp", cs_f, prev, precision=exact_prec)
    carried = carried * jnp.transpose(jnp.exp(cum), (1, 2, 0))[..., None]
    ssm = (inner + carried).reshape(length, heads_dev, head_dim)
    gated = (
        ssm + head_direct_scale[None, :, None] * xs_f.reshape(length, heads_dev, head_dim)
    ) * jax.nn.silu(output_gate_logits.astype(jnp.float32)).reshape(length, heads_dev, head_dim)
    gated = gated * lax.rsqrt(jnp.mean(gated * gated, axis=-1, keepdims=True) + eps)
    mixed = (gated.reshape(length, width) * gated_norm_scale.astype(jnp.float32)).astype(
        jnp.bfloat16
    )
    return lax.psum_scatter(
        jnp.dot(mixed, mixer_output_weight, preferred_element_type=jnp.float32).astype(
            jnp.bfloat16
        ),
        "tp",
        scatter_dimension=0,
        tiled=True,
    )


def expert_half(
    second_batch_tokens,
    pre_expert_norm_scale,
    group_router_columns,
    expert_router_columns,
    routes,
    expert_gate_weight,
    expert_up_weight,
    expert_down_weight,
):
    n_tok = second_batch_tokens.shape[0]
    n_tp = lax.axis_size("tp")
    n_experts = expert_router_columns.shape[1]
    capacity = 4 * n_tok // n_experts
    tokens_f = second_batch_tokens.astype(jnp.float32)
    normed = (
        tokens_f
        * lax.rsqrt(jnp.mean(tokens_f * tokens_f, axis=-1, keepdims=True) + eps)
        * pre_expert_norm_scale.astype(jnp.float32)
    ).astype(jnp.bfloat16)
    group_logits = jnp.dot(normed, group_router_columns, preferred_element_type=jnp.float32)
    expert_logits = jnp.dot(normed, expert_router_columns, preferred_element_type=jnp.float32)
    weights = route_weights(group_logits, expert_logits, routes)
    slots = routes * capacity + slot_positions(routes, n_experts).reshape(n_tok, 2)
    token_ids = jnp.repeat(jnp.arange(n_tok, dtype=jnp.int32), 2)
    source = (
        jnp.full((n_experts * capacity,), n_tok, jnp.int32).at[slots.reshape(-1)].set(token_ids)
    )
    padded = jnp.concatenate([normed, jnp.zeros((1, normed.shape[1]), jnp.bfloat16)], axis=0)
    outgoing = jnp.take(padded, source, axis=0).reshape(n_experts, capacity, normed.shape[1])
    share = capacity // n_tp
    own_share = lax.dynamic_slice_in_dim(outgoing, lax.axis_index("tp") * share, share, 1)
    arrived = lax.all_to_all(own_share, "ep", split_axis=0, concat_axis=0, tiled=True)
    rows = lax.all_gather(arrived, "tp", axis=1, tiled=True)
    gate = jnp.einsum(
        "skd,df->skf", rows, expert_gate_weight[0], preferred_element_type=jnp.float32
    )
    upper = jnp.einsum("skd,df->skf", rows, expert_up_weight[0], preferred_element_type=jnp.float32)
    hidden = (jax.nn.silu(gate) * upper).astype(jnp.bfloat16)
    n_src, slot_count, shard_width = hidden.shape
    flat = hidden.reshape(n_src * slot_count, shard_width)
    columns = expert_down_weight[0]
    summed = lax.psum_scatter(
        lax.dot_general(
            columns, flat, (((0,), (1,)), ((), ())), preferred_element_type=jnp.float32
        ).astype(jnp.bfloat16),
        "tp",
        scatter_dimension=0,
        tiled=True,
    ).astype(jnp.float32)
    going_back = summed.astype(jnp.bfloat16).reshape(summed.shape[0], n_src, slot_count)
    returned = lax.all_to_all(going_back, "ep", split_axis=1, concat_axis=1, tiled=True)
    flat_out = returned.reshape(returned.shape[0], -1).astype(jnp.float32)
    picked = jnp.take(flat_out, slots.reshape(-1), axis=1).reshape(flat_out.shape[0], n_tok, 2)
    combined = jnp.sum(picked * weights[None], axis=2)
    return jnp.transpose(combined).astype(jnp.bfloat16)


def per_device(
    mixer_input_channels,
    output_gate_logits,
    head_group_input_map,
    head_group_output_map,
    input_channel_taps,
    input_map_taps,
    output_map_taps,
    step_logits,
    head_log_rate,
    extra_log_decay,
    head_direct_scale,
    gated_norm_scale,
    mixer_output_weight,
    second_batch_tokens,
    pre_expert_norm_scale,
    group_router_columns,
    expert_router_columns,
    routes,
    expert_gate_weight,
    expert_up_weight,
    expert_down_weight,
):
    mixer_out = mixer_half(
        mixer_input_channels,
        output_gate_logits,
        head_group_input_map,
        head_group_output_map,
        input_channel_taps,
        input_map_taps,
        output_map_taps,
        step_logits,
        head_log_rate,
        extra_log_decay,
        head_direct_scale,
        gated_norm_scale,
        mixer_output_weight,
    )
    experts_out = expert_half(
        second_batch_tokens,
        pre_expert_norm_scale,
        group_router_columns,
        expert_router_columns,
        routes,
        expert_gate_weight,
        expert_up_weight,
        expert_down_weight,
    )
    return (mixer_out, experts_out)


def solution(mesh):
    in_specs = (
        P("ep", "tp"),
        P("ep", "tp"),
        P("ep", None),
        P("ep", None),
        P(None, "tp"),
        P(),
        P(),
        P("tp", "ep"),
        P("tp"),
        P("tp", "ep"),
        P("tp"),
        P("tp"),
        P("tp", None),
        P("ep", None),
        P(),
        P(),
        P(),
        P("ep", None),
        P("ep", None, "tp"),
        P("ep", None, "tp"),
        P("ep", "tp", None),
    )
    out_specs = (P(("ep", "tp"), None), P("ep", "tp"))
    return jax.shard_map(
        per_device, mesh=mesh, in_specs=in_specs, out_specs=out_specs, check_vma=False
    )
```

profile of v0, /device:TPU:1, one launch (start us, length us, event | category | flops | bytes accessed | tf_op | source)
XLA Modules:
  0.0 234.6 jit_solution(957158603250148099)
XLA Ops:
  7.2 0.9 copy.233
  8.5 1.2 reduce-window.6
  10.2 0.7 compare_and_fusion.1
  11.4 2.4 %scatter_custom_fusion = s32[1024]{0:T(1024)S(1)} fusion(s32[512]{0:T(512)S(1)} %bitcast.183, s32[512]{0:T(512)S(1)} %reshape.273, s32[]{:T(128)} %constant.106.clone.1), kind=kCustom, calls=%fused_computation.141 | custom fusion | bytes 4100 | tf_op jit(solution)/shard_map/scatter | solution.py:216
  13.9 0.7 convert_element_type.99
  15.4 6.0 %gather_fusion = bf16[1024,2048]{1,0:T(8,128)(2,1)} fusion(bf16[257,2048]{1,0:T(8,128)(2,1)S(1)} %concatenate.19, s32[1024]{0:T(1024)S(1)} %fusion.71), kind=kCustom, calls=%fused_computation | custom fusion | bytes 8392704 | tf_op jit(solution)/shard_map/jit(_take)/gather | solution.py:219
  21.5 1.2 dynamic-slice_select_fusion
  22.7 14.9 %all_to_all.15 = bf16[16,4,2048]{2,1,0:T(4,128)(2,1)S(1)} all-to-all(bf16[16,4,2048]{2,1,0:T(4,128)(2,1)S(1)} %dynamic-slice_select_fusion), channel_id=1, replica_groups=mesh['ep'=16,'tp'=16] {'ep'}, dimensions={0} | all-to-all | bytes 524288 | tf_op jit(solution)/shard_map/all_to_all | solution.py:222
  37.6 0.9 copy.239
  38.6 1.6 constant_dynamic-slice_fusion.1
  40.6 1.2 copy.216
  41.9 2.7 %collective-permute-start = (bf16[3,256]{0,1:T(8,128)(2,1)S(1)}, bf16[3,256]{0,1:T(8,128)(2,1)S(1)}, u32[]{:S(2)}, u32[]{:S(2)}) collective-permute-start(bf16[3,256]{0,1:T(8,128)(2,1)S(1)} %pad_maximum_fusion), channel_id=1, source_target_pairs={{0,16},{16,32},{32,48},{48,64},{64,80},{80,96},{96,112},{112,128},... | collective-permute-start | bytes 4616 | tf_op jit(solution)/shard_map/ppermute | solution.py:19
  45.9 35.5 %all-gather.2.cloned.1.call-done = bf16[16,64,2048]{2,0,1:T(8,128)(2,1)} async-done(((bf16[16,4,2048]{2,0,1:T(8,128)(2,1)}), bf16[16,64,2048]{2,0,1:T(8,128)(2,1)}) %all-gather.2.cloned.1.call-update) | async-done | bytes 4194320 | tf_op jit(solution)/shard_map/all_gather | solution.py:223
  81.4 3.9 %fusion.34 = f32[16,64,256]{2,0,1:T(8,128)S(1)} fusion(bf16[16,64,2048]{2,0,1:T(8,128)(2,1)} %all-gather.2.cloned.1.call-done, bf16[1,2048,256]{2,1,0:T(8,128)(2,1)} %param.39), kind=kOutput, calls=%fused_computation.50 | convolution fusion | flops 1073741824 | bytes 6291456 | tf_op jit(solution)/shard_map/skd,df->skf/dot_general | solution.py:224
  85.4 1.3 fusion.20
  86.9 3.2 %convert_bitcast_fusion = bf16[2048,1024]{0,1:T(8,128)(2,1)} fusion(bf16[1024,256]{1,0:T(8,128)(2,1)S(1)} %bitcast.175, bf16[1,256,2048]{2,1,0:T(8,128)(2,1)S(1)} %copy-done), kind=kOutput, calls=%fused_computation.5 | convolution fusion | flops 1075838976 | bytes 5767168 | tf_op jit(solution)/shard_map/dot_general | solution.py:233
  90.1 6.4 %copy.252 = bf16[2048,1024]{1,0:T(8,128)(2,1)} copy(bf16[2048,1024]{0,1:T(8,128)(2,1)} %convert_bitcast_fusion) | data formatting | bytes 8388608
  97.8 2.0 copy.231
  100.4 2.1 multiply_convert_fusion
  102.8 1.0 slice_bitcast_fusion.2
  103.8 1.1 broadcast_multiply_fusion
  105.0 0.9 fusion.37
  105.9 1.0 copy-done.1
  106.9 1.2 fusion.45
  108.3 0.8 broadcast_in_dim.148
  109.1 6.6 %all-to-all-start = ((bf16[16,129,64]{1,2,0:T(8,128)(2,1)}), bf16[16,129,64]{1,2,0:T(8,128)(2,1)}, u32[]{:S(2)}, u32[]{:S(2)}) async-start(bf16[16,129,64]{1,2,0:T(8,128)(2,1)} %broadcast_in_dim.148), calls=%async_computation | async-start | bytes 1048576 | tf_op jit(solution)/shard_map/all_to_all | solution.py:24
  116.0 1.0 copy.264
  117.0 2.4 %fusion.49 = f32[16,128,128]{2,1,0:T(8,128)} fusion(bf16[8,16,8,128]{3,2,1,0:T(8,128)(2,1)} %get-tuple-element.7, bf16[8,16,8,128]{3,2,1,0:T(8,128)(2,1)} %get-tuple-element.6), kind=kOutput, calls=%fused_computation.70 | convolution fusion | flops 33554432 | bytes 1572864 | tf_op jit(solution)/shard_map/bln,bsn->bls/dot_general | solution.py:147
  119.4 7.2 %all-to-all-done = bf16[16,129,64]{1,2,0:T(8,128)(2,1)} async-done(((bf16[16,129,64]{1,2,0:T(8,128)(2,1)}), bf16[16,129,64]{1,2,0:T(8,128)(2,1)}, u32[]{:S(2)}, u32[]{:S(2)}) %all-to-all-start) | async-done | bytes 264224 | tf_op jit(solution)/shard_map/all_to_all | solution.py:24
  126.6 1.7 slice.157
  128.3 1.1 copy.256
  129.6 1.8 slice_convert_fusion.1
  131.4 2.4 %copy.251 = f32[16,128,64]{2,1,0:T(8,128)} copy(f32[16,128,64]{1,2,0:T(8,128)} %slice_convert_fusion.1) | data formatting | bytes 1048576 | tf_op jit(solution)/shard_map/convert_element_type | solution.py:61
  133.8 1.5 broadcast_select_fusion
  135.7 1.6 fusion.19
  137.3 0.9 convolution_multiply_fusion.1
  138.3 4.6 %fusion.16 = f32[16,128,2,64]{1,3,2,0:T(8,128)S(1)} fusion(f32[16,128,2,64]{1,3,2,0:T(8,128)S(1)} %convolution_multiply_fusion.1, f32[16,128,2,64]{1,0,3,2:T(8,128)S(1)} %copy-done.5, f32[16,128,128]{2,1,0:T(8,128)S(1)} %copy-done.6, f32[2,16,128]{2,0,1:T(2,128)S(1)} %copy.212, pred[128,128]{1,0:T(8,128)(4,1)S(1)} %iota_compare_fusion), kind=kOutput, calls=%fused_computation.26 | convolution fusion | flops 405012480 | bytes 4227072 | tf_op jit(solution)/shard_map/bls,hbls,bshp->blhp/dot_general | solution.py:148
  142.9 0.6 copy.230
  144.5 0.8 fusion.28
  145.3 5.6 %convolution_convert_fusion = bf16[2048,2048]{1,0:T(8,128)(2,1)} fusion(bf16[2048,128]{0,1:T(8,128)(2,1)S(1)} %fusion.28, bf16[128,2048]{1,0:T(8,128)(2,1)S(1)} %copy-done.7), kind=kOutput, calls=%fused_computation.4 | convolution fusion | flops 1077936128 | bytes 9437184 | tf_op jit(solution)/shard_map/dot_general | solution.py:181
  150.9 0.7 copy-done.10
  152.7 3.0 %reduce-scatter.7.cloned.1.call-done = bf16[128,1024]{1,0:T(8,128)(2,1)} async-done(((bf16[2048,1024]{1,0:T(8,128)(2,1)}), bf16[128,1024]{1,0:T(8,128)(2,1)}) %reduce-scatter.7.cloned.1.call-update) | async-done | bytes 262160
  155.7 1.8 copy.253
  157.5 6.4 %all-to-all-start.2 = ((bf16[128,16,64]{0,2,1:T(8,128)(2,1)}), bf16[128,16,64]{0,2,1:T(8,128)(2,1)S(1)}, u32[]{:S(2)}, u32[]{:S(2)}) async-start(bf16[128,16,64]{0,2,1:T(8,128)(2,1)} %bitcast.36), calls=%async_computation.3 | async-start | bytes 524288 | tf_op jit(solution)/shard_map/all_to_all | solution.py:241
  164.2 7.2 %all-to-all-done.2 = bf16[128,16,64]{0,2,1:T(8,128)(2,1)S(1)} async-done(((bf16[128,16,64]{0,2,1:T(8,128)(2,1)}), bf16[128,16,64]{0,2,1:T(8,128)(2,1)S(1)}, u32[]{:S(2)}, u32[]{:S(2)}) %all-to-all-start.2) | async-done | bytes 262176 | tf_op jit(solution)/shard_map/all_to_all | solution.py:241
  171.5 1.0 gather_fusion.1
  172.5 2.1 multiply_reduce_fusion
  174.6 53.5 %reduce-scatter.5.cloned.1.call-done = bf16[128,2048]{1,0:T(8,128)(2,1)} async-done(((bf16[2048,2048]{1,0:T(8,128)(2,1)}), bf16[128,2048]{1,0:T(8,128)(2,1)}) %reduce-scatter.5.cloned.1.call-update) | async-done | bytes 524304 | tf_op jit(solution)/shard_map/reduce_scatter | solution.py:180
  (145 shorter events, 9.9 us)
Async XLA Ops:
  7.2 79.7 %copy-start = (bf16[1,256,2048]{2,1,0:T(8,128)(2,1)S(1)}, bf16[1,256,2048]{2,1,0:T(8,128)(2,1)}, u32[]{:S(2)}) copy-start(bf16[1,256,2048]{2,1,0:T(8,128)(2,1)} %param.41) | copy-start | bytes 3145732
  7.2 7.4 %copy-start.4 = (bf16[256,2048]{1,0:T(8,128)(2,1)S(1)}, bf16[256,2048]{1,0:T(8,128)(2,1)}, u32[]{:S(2)}) copy-start(bf16[256,2048]{1,0:T(8,128)(2,1)} %param.34) | copy-start | bytes 3145732
  7.2 74.2 %all-gather.2.cloned.1.call-start = ((), (), s32[]{:S(2)}) async-start(), calls=%async_computation.6 | async-start | bytes 4456448 | tf_op jit(solution)/shard_map/all_gather | solution.py:223
  38.5 117.2 %reduce-scatter.7.cloned.1.call-start = ((), (), s32[]{:S(2)}) async-start(), calls=%async_computation.7 | async-start | bytes 4456448
  40.1 4.5 %copy-start.19 = (f32[2]{0:T(128)S(1)}, f32[2]{0:T(128)}, u32[]{:S(2)}) copy-start(f32[2]{0:T(128)} %param.29) | copy-start | bytes 28
  40.1 4.5 %copy-start.11 = (f32[2,2048]{1,0:T(2,128)S(1)}, f32[2,2048]{1,0:T(2,128)}, u32[]{:S(2)}) copy-start(f32[2,2048]{1,0:T(2,128)} %param.28) | copy-start | bytes 49156
  40.1 4.5 %copy-start.12 = (f32[2,2048]{1,0:T(2,128)S(1)}, f32[2,2048]{1,0:T(2,128)}, u32[]{:S(2)}) copy-start(f32[2,2048]{1,0:T(2,128)} %param.30) | copy-start | bytes 49156
  41.9 58.1 %collective-permute-start = (bf16[3,256]{0,1:T(8,128)(2,1)S(1)}, bf16[3,256]{0,1:T(8,128)(2,1)S(1)}, u32[]{:S(2)}, u32[]{:S(2)}) collective-permute-start(bf16[3,256]{0,1:T(8,128)(2,1)S(1)} %pad_maximum_fusion), channel_id=1, source_target_pairs={{0,16},{16,32},{32,48},{48,64},{64,80},{80,96},{96,112},{112,128},... | collective-permute-start | bytes 4616 | tf_op jit(solution)/shard_map/ppermute | solution.py:19
  81.4 3.9 %copy-start.17 = (bf16[16,64,2048]{2,0,1:T(8,128)(2,1)S(1)}, bf16[16,64,2048]{2,0,1:T(8,128)(2,1)}, u32[]{:S(2)}) copy-start(bf16[16,64,2048]{2,0,1:T(8,128)(2,1)} %all-gather.2.cloned.1.call-done) | copy-start | bytes 12582916
  81.4 4.1 %copy-start.18 = (bf16[1,2048,256]{2,1,0:T(8,128)(2,1)S(1)}, bf16[1,2048,256]{2,1,0:T(8,128)(2,1)}, u32[]{:S(2)}) copy-start(bf16[1,2048,256]{2,1,0:T(8,128)(2,1)} %param.40) | copy-start | bytes 3145732
  96.5 0.7 copy-start.15
  96.5 0.7 copy-start.16
  96.5 0.8 copy-start.13
  96.5 3.4 %copy-start.14 = (f32[2]{0:T(128)S(1)}, f32[2]{0:T(128)}, u32[]{:S(2)}) copy-start(f32[2]{0:T(128)} %param.31) | copy-start | bytes 28
  96.5 3.5 %copy-start.20 = (bf16[128]{0:T(256)(128)(2,1)S(1)}, bf16[128]{0:T(256)(128)(2,1)}, u32[]{:S(2)}) copy-start(bf16[128]{0:T(256)(128)(2,1)} %param.32) | copy-start | bytes 772
  105.9 1.0 copy-start.1
  109.1 17.5 %all-to-all-start = ((bf16[16,129,64]{1,2,0:T(8,128)(2,1)}), bf16[16,129,64]{1,2,0:T(8,128)(2,1)}, u32[]{:S(2)}, u32[]{:S(2)}) async-start(bf16[16,129,64]{1,2,0:T(8,128)(2,1)} %broadcast_in_dim.148), calls=%async_computation | async-start | bytes 1048576 | tf_op jit(solution)/shard_map/all_to_all | solution.py:24
  115.7 112.4 %reduce-scatter.5.cloned.1.call-start = ((), (), s32[]{:S(2)}) async-start(), calls=%async_computation.5 | async-start | bytes 8912896 | tf_op jit(solution)/shard_map/reduce_scatter | solution.py:180
  133.8 1.9 copy-start.2
  135.7 2.6 %copy-start.5 = (f32[16,128,2,64]{1,0,3,2:T(8,128)S(1)}, f32[16,128,2,64]{1,0,3,2:T(8,128)}, u32[]{:S(2)}) copy-start(f32[16,128,2,64]{1,0,3,2:T(8,128)} %get-tuple-element.5) | copy-start | bytes 3145732
  135.7 2.6 %copy-start.6 = (f32[16,128,128]{2,1,0:T(8,128)S(1)}, f32[16,128,128]{2,1,0:T(8,128)}, u32[]{:S(2)}) copy-start(f32[16,128,128]{2,1,0:T(8,128)} %fusion.49) | copy-start | bytes 3145732
  142.9 1.0 copy-start.3
  143.9 1.3 copy-start.7
  150.9 0.7 copy-start.10
  150.9 1.2 copy-start.8
  151.6 1.0 copy-start.9
  157.5 13.9 %all-to-all-start.2 = ((bf16[128,16,64]{0,2,1:T(8,128)(2,1)}), bf16[128,16,64]{0,2,1:T(8,128)(2,1)S(1)}, u32[]{:S(2)}, u32[]{:S(2)}) async-start(bf16[128,16,64]{0,2,1:T(8,128)(2,1)} %bitcast.36), calls=%async_computation.3 | async-start | bytes 524288 | tf_op jit(solution)/shard_map/all_to_all | solution.py:241
Sparse Core Ops, SparseCore 0:
  38.6 42.7 all-gather.1
  96.7 58.9 reduce-scatter.6
  158.8 69.2 reduce-scatter.4
where the time goes:
time: 238 us; the launch traced here: 235 us
  waiting for transfers between devices  106 us (45%)
  local copies, waits for them, and re-layouts  39.6 us (17%)
  matrix products  26.3 us (11%)
  other arithmetic  17 us (7%)
  starting transfers between devices  16 us (7%)
  blocking collectives  14.9 us (6%)
  between operations  14.5 us (6%)
    reduce_scatter x1, waiting for transfers between devices, mixer_half(): lax.psum_scatter(jnp.dot(mixed, mixer_output_weight, preferred_element_ty...  53.5 us
    all_gather x1, waiting for transfers between devices, expert_half(): rows = lax.all_gather(arrived, 'tp', axis=1, tiled=True)  35.5 us
    unnamed x54, local copies, waits for them, and re-layouts  19.1 us
    all_to_all x1, blocking collectives, expert_half(): lax.all_to_all(own_share, 'ep', split_axis=0, concat_axis=0, tiled=True)  14.9 us
    all_to_all x1, waiting for transfers between devices, from_everyone(): lax.all_to_all(jnp.broadcast_to(value[None], (size, *value.shape)), axis,...  7.23 us
    all_to_all x1, waiting for transfers between devices, expert_half(): lax.all_to_all(going_back, 'ep', split_axis=1, concat_axis=1, tiled=True)  7.18 us
    all_to_all x1, starting transfers between devices, from_everyone(): lax.all_to_all(jnp.broadcast_to(value[None], (size, *value.shape)), axis,...  6.58 us
    all_to_all x1, starting transfers between devices, expert_half(): lax.all_to_all(going_back, 'ep', split_axis=1, concat_axis=1, tiled=True)  6.39 us
  transfers between devices with their start and end apart: 6, of which 5 were waited for; matrix products, arithmetic and copies ran while one was open for 27% of the time, Pallas kernels for 0%

commit v1 on v0

--- a/solution.py
+++ b/solution.py
@@ -1,6 +1,8 @@
 import jax
 import jax.numpy as jnp
 from jax import lax
+from jax.experimental import pallas as pl
+from jax.experimental.pallas import tpu as pltpu
 from jax.sharding import PartitionSpec as P
 
 HEADS = 32
@@ -8,9 +10,323 @@
 GROUPS = 4
 BLOCK = 128
 
-
 eps = 1e-06
 exact_prec = lax.Precision.HIGHEST
+bf16, f32 = jnp.bfloat16, jnp.float32
+
+NEP = 16
+NZ = 8
+CAP = 64
+HALF = CAP // 2
+ORDER = (4, 3, 5, 2, 6, 1, 7, 0)
+
+
+def kernel(
+    tok, nsc, rg, re, rt, gate_h, up_h, down_h, mixed_h, w_h,
+    mo, eo,
+    nrm, sbuf, xr, gw, uw, dn, hall, ysend, ybuf, zsend, zbuf, wg, mx, psend, precv,
+    loc_s, dnl_s, dns_s, dnr_s, xs_s, xr_s, xf_s, xg_s, hs_s, hr_s, ys_s, yr_s, zs_s, zr_s,
+    ws_s, wr_s, ms_s, mr_s, fs_s, fr_s,
+):
+    ep, tp = lax.axis_index("ep"), lax.axis_index("tp")
+    y, x = ep // 4, ep % 4
+    z, c = tp // 2, tp % 2
+    other = z * 2 + (1 - c)
+
+    def ep_at(d, sign):
+        return ((y + 4 + sign * (d // 4)) % 4) * 4 + (x + 4 + sign * (d % 4)) % 4
+
+    def tp_at(r):
+        return ((z + r) % NZ) * 2 + c
+
+    def push(src, dst, ss, rs, e, t):
+        return pltpu.make_async_remote_copy(
+            src_ref=src, dst_ref=dst, send_sem=ss, recv_sem=rs,
+            device_id={"ep": e, "tp": t}, device_id_type=pl.DeviceIdType.MESH,
+        )
+
+    barrier = pltpu.get_barrier_semaphore()
+
+    def greet(e, t):
+        pl.semaphore_signal(
+            barrier, inc=1, device_id={"ep": e, "tp": t}, device_id_type=pl.DeviceIdType.MESH
+        )
+
+    lg = pltpu.make_async_copy(gate_h, gw, loc_s.at[0])
+    lu = pltpu.make_async_copy(up_h, uw, loc_s.at[1])
+    lw = pltpu.make_async_copy(w_h, wg.at[pl.ds(0, 128), :], loc_s.at[2])
+    lm = pltpu.make_async_copy(
+        mixed_h.at[pl.ds(pl.multiple_of(z * 256, 256), 256), :], mx.at[:, pl.ds(0, 128)], loc_s.at[3]
+    )
+    for cp in (lg, lu, lw, lm):
+        cp.start()
+
+    def down_cols(q, core):
+        return down_h.at[:, pl.ds(pl.multiple_of((2 * ((z + ORDER[q]) % NZ) + core) * 128, 128), 128)]
+
+    dn_l = [
+        pltpu.make_async_copy(
+            down_cols(q, c), dn.at[c, :, pl.ds(q * 128, 128)], dnl_s.at[q]
+        )
+        for q in range(NZ)
+    ]
+    for cp in dn_l:
+        cp.start()
+
+    for d in range(1, NEP):
+        greet(ep_at(d, 1), tp)
+    for r in range(1, NZ):
+        greet(ep, tp_at(r))
+    greet(ep, other)
+    pl.semaphore_wait(barrier, NEP - 1 + NZ - 1 + 1)
+
+    dn_r = [
+        push(down_cols(q, 1 - c), dn.at[c, :, pl.ds(q * 128, 128)], dns_s.at[q], dnr_s.at[q], ep, other)
+        for q in range(NZ)
+    ]
+    for cp in dn_r:
+        cp.start()
+    m_cp = [
+        push(
+            mixed_h.at[pl.ds(pl.multiple_of(((z + r) % NZ) * 256, 256), 256), :],
+            mx.at[:, pl.ds((NZ - r) * 128, 128)],
+            ms_s.at[NZ - r], mr_s.at[NZ - r], ep, tp_at(r),
+        )
+        for r in (4, 3, 5, 2, 6, 1, 7)
+    ]
+    for cp in m_cp:
+        cp.start()
+
+    def w_copy(way, k):
+        if way == 0:
+            a, b, t = (9 - k) % NZ, NZ - k, tp_at(1)
+        else:
+            a, b, t = k - 1, k, tp_at(NZ - 1)
+        lo, n = (0, 128) if k < 4 else (64 * way, 64)
+        src = w_h.at[pl.ds(lo, n), :] if k == 1 else wg.at[pl.ds(a * 128 + lo, n), :]
+        return push(
+            src, wg.at[pl.ds(b * 128 + lo, n), :], ws_s.at[way, k - 1], wr_s.at[way, k - 1], ep, t
+        )
+
+    w_cp = [[w_copy(way, k) for k in range(1, 5)] for way in range(2)]
+
+    def w_step(k):
+        for way in range(2):
+            if k > 1:
+                w_cp[way][k - 2].wait_recv()
+            w_cp[way][k - 1].start()
+
+    w_step(1)
+
+    def norm_rows(i, _):
+        rows = pl.ds(pl.multiple_of(i * 32, 32), 32)
+        v = tok[rows, :].astype(f32)
+        v = v * lax.rsqrt(jnp.mean(v * v, axis=1, keepdims=True) + eps) * nsc[...].astype(f32)
+        nrm[rows, :] = v.astype(bf16)
+        return 0
+
+    lax.fori_loop(0, 8, norm_rows, 0)
+
+    r0, r1 = rt[0:1, :], rt[1:2, :]
+    di = lax.broadcasted_iota(jnp.int32, (NEP, 256), 0)
+    e_rel = (((y + lax.shift_right_logical(di, 2)) & 3) * 4) + ((x + di) & 3)
+    in0, in1 = e_rel == r0, e_rel == r1
+    routed = in0 | in1
+    onehot = jnp.where(routed, 1.0, 0.0).astype(bf16)
+    a = lax.broadcasted_iota(jnp.int32, (256, 256), 0)
+    b = lax.broadcasted_iota(jnp.int32, (256, 256), 1)
+    before = jnp.where(a < b, 1.0, 0.0).astype(bf16)
+    place = jnp.dot(onehot, before, preferred_element_type=f32)
+    place = jnp.where(routed, place, -1.0)
+    slot = lax.broadcasted_iota(jnp.int32, (HALF, 256), 0) + HALF * c
+    slot = slot.astype(f32)
+    tokens_n = nrm[...]
+    for q in range(4):
+        pick = jnp.concatenate(
+            [jnp.where(place[d : d + 1, :] == slot, 1.0, 0.0) for d in range(4 * q, 4 * q + 4)], axis=0
+        ).astype(bf16)
+        sbuf[q * 128 : (q + 1) * 128, :] = jnp.dot(pick, tokens_n, preferred_element_type=f32).astype(bf16)
+    x_cp = [
+        push(
+            sbuf.at[pl.ds(d * HALF, HALF), :],
+            xr.at[pl.ds(pl.multiple_of(d * CAP + HALF * c, HALF), HALF), :],
+            xs_s.at[d], xr_s.at[d], ep_at(d, 1), tp,
+        )
+        for d in range(1, NEP)
+    ]
+    for cp in x_cp:
+        cp.start()
+    xr[pl.ds(pl.multiple_of(HALF * c, HALF), HALF), :] = sbuf[0:HALF, :]
+
+    nt = (((1,), (1,)), ((), ()))
+    gl = lax.dot_general(rg[...], tokens_n, nt, preferred_element_type=f32)
+    el = lax.dot_general(re[...], tokens_n, nt, preferred_element_type=f32)
+
+    def lse(v):
+        top = jnp.max(v, axis=0, keepdims=True)
+        return top + jnp.log(jnp.sum(jnp.exp(v - top), axis=0, keepdims=True))
+
+    gl = gl - lse(gl)
+    ei = lax.broadcasted_iota(jnp.int32, (4, 256), 0)
+    lp0 = jnp.zeros((1, 256), f32)
+    lp1 = jnp.zeros((1, 256), f32)
+    for g in range(4):
+        part = el[4 * g : 4 * g + 4, :]
+        part = part - lse(part) + gl[g : g + 1, :]
+        lp0 += jnp.sum(jnp.where(ei + 4 * g == r0, part, 0.0), axis=0, keepdims=True)
+        lp1 += jnp.sum(jnp.where(ei + 4 * g == r1, part, 0.0), axis=0, keepdims=True)
+    top = jnp.maximum(lp0, lp1)
+    w0, w1 = jnp.exp(lp0 - top), jnp.exp(lp1 - top)
+    total = w0 + w1
+    share = jnp.where(in0, w0 / total, 0.0) + jnp.where(in1, w1 / total, 0.0)
+    both = jnp.concatenate([place, share, jnp.zeros((96, 256), f32)], axis=0).T
+
+    lane = lax.broadcasted_iota(jnp.int32, (256, 128), 1)
+    in_slot = (lane & (CAP - 1)).astype(f32)
+    low = lane < CAP
+    mixw = []
+    for p in range(8):
+        at = jnp.where(low, both[:, 2 * p : 2 * p + 1], both[:, 2 * p + 1 : 2 * p + 2])
+        sh = jnp.where(low, both[:, 16 + 2 * p : 17 + 2 * p], both[:, 17 + 2 * p : 18 + 2 * p])
+        mixw.append(jnp.where(at == in_slot, sh, 0.0).astype(bf16))
+    mixw = jnp.concatenate(mixw, axis=1)
+
+    lg.wait()
+    lu.wait()
+    for cp in dn_l:
+        cp.wait()
+
+    def x_hand(d):
+        rows = pl.ds(pl.multiple_of(d * CAP + HALF * c, HALF), HALF)
+        return push(xr.at[rows, :], xr.at[rows, :], xf_s.at[d], xg_s.at[d], ep, other)
+
+    hand = [x_hand(d) for d in range(NEP)]
+
+    def y_copy(d, h):
+        part = (pl.ds(d * CAP, CAP), pl.ds(h * 512, 512))
+        return push(ysend.at[part], ybuf.at[part], ys_s.at[h, d], yr_s.at[h, d], ep_at(d, -1), tp)
+
+    y_cp = [[y_copy(d, h) for d in range(1, NEP)] for h in range(2)]
+    h_cp = []
+    for g in range(4):
+        for d in range(4 * g, 4 * g + 4):
+            if d > 0:
+                x_cp[d - 1].wait_recv()
+            hand[d].start()
+        for d in range(4 * g, 4 * g + 4):
+            hand[d].wait_recv()
+        rows = slice(256 * g, 256 * (g + 1))
+        xg = xr[rows, :]
+        gv = jnp.dot(xg, gw[...], preferred_element_type=f32)
+        uv = jnp.dot(xg, uw[...], preferred_element_type=f32)
+        hall[c, rows, :] = (gv * jax.nn.sigmoid(gv) * uv).astype(bf16)
+        part = hall.at[c, pl.ds(256 * g, 256), :]
+        cp = push(part, part, hs_s.at[g], hr_s.at[g], ep, other)
+        cp.start()
+        h_cp.append(cp)
+        if g == 0:
+            for cq in dn_r:
+                cq.wait_recv()
+        if g == 1:
+            w_step(2)
+        cp.wait_recv()
+        yv = jnp.dot(hall[0, rows, :], dn[0], preferred_element_type=f32)
+        yv += jnp.dot(hall[1, rows, :], dn[1], preferred_element_type=f32)
+        ysend[rows, :] = yv.astype(bf16)
+        for d in range(4 * g, 4 * g + 4):
+            if d > 0:
+                y_cp[0][d - 1].start()
+    for d in range(1, NEP):
+        y_cp[1][d - 1].start()
+    ybuf[0:CAP, :] = ysend[0:CAP, :]
+    w_step(3)
+
+    z_cp = []
+    for h in range(2):
+        for d in range(1, NEP):
+            y_cp[h][d - 1].wait_recv()
+        cols = slice(512 * h, 512 * (h + 1))
+        comb = jnp.dot(mixw, ybuf[:, cols], preferred_element_type=f32)
+        for i in range(4):
+            r = ORDER[4 * h + i]
+            val = comb[:, 128 * i : 128 * (i + 1)]
+            if r == 0:
+                zbuf[0] = val.astype(bf16)
+                continue
+            zsend[r] = val.astype(bf16)
+            cp = push(zsend.at[r], zbuf.at[NZ - r], zs_s.at[NZ - r], zr_s.at[NZ - r], ep, tp_at(r))
+            cp.start()
+            z_cp.append(cp)
+        if h == 0:
+            w_step(4)
+
+    lw.wait()
+    lm.wait()
+    for cp in m_cp:
+        cp.wait_recv()
+    for way in range(2):
+        w_cp[way][3].wait_recv()
+    theirs = mx[pl.ds(pl.multiple_of((1 - c) * 128, 128), 128), :]
+    psend[...] = jnp.dot(theirs, wg[...], preferred_element_type=f32).astype(bf16)
+    fin = push(psend, precv, fs_s, fr_s, ep, other)
+    fin.start()
+    ours = mx[pl.ds(pl.multiple_of(c * 128, 128), 128), :]
+    mine = jnp.dot(ours, wg[...], preferred_element_type=f32)
+    fin.wait_recv()
+    mo[...] = (mine + precv[...].astype(f32)).astype(bf16)
+
+    acc = zbuf[0].astype(f32)
+    for cp in z_cp:
+        cp.wait_recv()
+    for r in range(1, NZ):
+        acc += zbuf[r].astype(f32)
+    eo[...] = acc.astype(bf16)
+
+    for cp in dn_r + m_cp + x_cp + hand + y_cp[0] + y_cp[1] + h_cp + z_cp + [fin]:
+        cp.wait_send()
+    for way in range(2):
+        for cp in w_cp[way]:
+            cp.wait_send()
+
+
+def fused(tok, nsc, rg, re, rt, gate, up, down, mixed, w):
+    vmem, hbm = pl.BlockSpec(memory_space=pltpu.VMEM), pl.BlockSpec(memory_space=pl.ANY)
+    dma = pltpu.SemaphoreType.DMA
+    v = pltpu.VMEM
+    return pl.pallas_call(
+        kernel,
+        out_shape=(
+            jax.ShapeDtypeStruct((128, 2048), bf16),
+            jax.ShapeDtypeStruct((256, 128), bf16),
+        ),
+        in_specs=[vmem] * 5 + [hbm] * 5,
+        out_specs=(vmem, vmem),
+        scratch_shapes=[
+            v((256, 2048), bf16),
+            v((512, 2048), bf16),
+            v((1024, 2048), bf16),
+            v((2048, 256), bf16),
+            v((2048, 256), bf16),
+            v((2, 256, 1024), bf16),
+            v((2, 1024, 256), bf16),
+            v((1024, 1024), bf16),
+            v((1024, 1024), bf16),
+            v((8, 256, 128), bf16),
+            v((8, 256, 128), bf16),
+            v((1024, 2048), bf16),
+            v((256, 1024), bf16),
+            v((128, 2048), bf16),
+            v((128, 2048), bf16),
+            dma((4,)), dma((8,)), dma((8,)), dma((8,)),
+            dma((16,)), dma((16,)), dma((16,)), dma((16,)),
+            dma((4,)), dma((4,)), dma((2, 16)), dma((2, 16)),
+            dma((8,)), dma((8,)), dma((2, 4)), dma((2, 4)), dma((8,)), dma((8,)),
+            dma, dma,
+        ],
+        compiler_params=pltpu.CompilerParams(
+            collective_id=0, has_side_effects=True, vmem_limit_bytes=56 * 1024 * 1024
+        ),
+    )(tok, nsc, rg, re, rt, gate, up, down, mixed, w)
 
 
 def from_behind(value, axis, steps):
@@ -81,26 +397,6 @@
 
 def chain_states(earlier, later):
     return (earlier[0] * later[1][:, None, None] + later[0], earlier[1] * later[1])
-
-
-def slot_positions(route_rows, n_experts):
-    flat = route_rows.reshape(-1)
-    onehot = (flat[:, None] == jnp.arange(n_experts, dtype=jnp.int32)[None, :]).astype(jnp.int32)
-    return jnp.sum(onehot * jnp.cumsum(onehot, axis=0), axis=1) - 1
-
-
-def route_weights(group_logits, expert_logits, routes):
-    n_groups = group_logits.shape[1]
-    n_experts = expert_logits.shape[1]
-    per_group = n_experts // n_groups
-    group_lp = jax.nn.log_softmax(group_logits, axis=-1)
-    inner_lp = jax.nn.log_softmax(expert_logits.reshape(-1, n_groups, per_group), axis=-1).reshape(
-        -1, n_experts
-    )
-    total = jnp.repeat(group_lp, per_group, axis=1) + inner_lp
-    pick = routes[:, :, None] == jnp.arange(n_experts, dtype=jnp.int32)[None, None, :]
-    chosen = jnp.sum(jnp.where(pick, total[:, None, :], 0.0), axis=-1)
-    return jax.nn.softmax(chosen, axis=-1)
 
 
 def mixer_half(
@@ -177,72 +473,7 @@
     mixed = (gated.reshape(length, width) * gated_norm_scale.astype(jnp.float32)).astype(
         jnp.bfloat16
     )
-    return lax.psum_scatter(
-        jnp.dot(mixed, mixer_output_weight, preferred_element_type=jnp.float32).astype(
-            jnp.bfloat16
-        ),
-        "tp",
-        scatter_dimension=0,
-        tiled=True,
-    )
-
-
-def expert_half(
-    second_batch_tokens,
-    pre_expert_norm_scale,
-    group_router_columns,
-    expert_router_columns,
-    routes,
-    expert_gate_weight,
-    expert_up_weight,
-    expert_down_weight,
-):
-    n_tok = second_batch_tokens.shape[0]
-    n_tp = lax.axis_size("tp")
-    n_experts = expert_router_columns.shape[1]
-    capacity = 4 * n_tok // n_experts
-    tokens_f = second_batch_tokens.astype(jnp.float32)
-    normed = (
-        tokens_f
-        * lax.rsqrt(jnp.mean(tokens_f * tokens_f, axis=-1, keepdims=True) + eps)
-        * pre_expert_norm_scale.astype(jnp.float32)
-    ).astype(jnp.bfloat16)
-    group_logits = jnp.dot(normed, group_router_columns, preferred_element_type=jnp.float32)
-    expert_logits = jnp.dot(normed, expert_router_columns, preferred_element_type=jnp.float32)
-    weights = route_weights(group_logits, expert_logits, routes)
-    slots = routes * capacity + slot_positions(routes, n_experts).reshape(n_tok, 2)
-    token_ids = jnp.repeat(jnp.arange(n_tok, dtype=jnp.int32), 2)
-    source = (
-        jnp.full((n_experts * capacity,), n_tok, jnp.int32).at[slots.reshape(-1)].set(token_ids)
-    )
-    padded = jnp.concatenate([normed, jnp.zeros((1, normed.shape[1]), jnp.bfloat16)], axis=0)
-    outgoing = jnp.take(padded, source, axis=0).reshape(n_experts, capacity, normed.shape[1])
-    share = capacity // n_tp
-    own_share = lax.dynamic_slice_in_dim(outgoing, lax.axis_index("tp") * share, share, 1)
-    arrived = lax.all_to_all(own_share, "ep", split_axis=0, concat_axis=0, tiled=True)
-    rows = lax.all_gather(arrived, "tp", axis=1, tiled=True)
-    gate = jnp.einsum(
-        "skd,df->skf", rows, expert_gate_weight[0], preferred_element_type=jnp.float32
-    )
-    upper = jnp.einsum("skd,df->skf", rows, expert_up_weight[0], preferred_element_type=jnp.float32)
-    hidden = (jax.nn.silu(gate) * upper).astype(jnp.bfloat16)
-    n_src, slot_count, shard_width = hidden.shape
-    flat = hidden.reshape(n_src * slot_count, shard_width)
-    columns = expert_down_weight[0]
-    summed = lax.psum_scatter(
-        lax.dot_general(
-            columns, flat, (((0,), (1,)), ((), ())), preferred_element_type=jnp.float32
-        ).astype(jnp.bfloat16),
-        "tp",
-        scatter_dimension=0,
-        tiled=True,
-    ).astype(jnp.float32)
-    going_back = summed.astype(jnp.bfloat16).reshape(summed.shape[0], n_src, slot_count)
-    returned = lax.all_to_all(going_back, "ep", split_axis=1, concat_axis=1, tiled=True)
-    flat_out = returned.reshape(returned.shape[0], -1).astype(jnp.float32)
-    picked = jnp.take(flat_out, slots.reshape(-1), axis=1).reshape(flat_out.shape[0], n_tok, 2)
-    combined = jnp.sum(picked * weights[None], axis=2)
-    return jnp.transpose(combined).astype(jnp.bfloat16)
+    return mixed
 
 
 def per_device(
@@ -268,7 +499,7 @@
     expert_up_weight,
     expert_down_weight,
 ):
-    mixer_out = mixer_half(
+    mixed = mixer_half(
         mixer_input_channels,
         output_gate_logits,
         head_group_input_map,
@@ -283,17 +514,18 @@
         gated_norm_scale,
         mixer_output_weight,
     )
-    experts_out = expert_half(
+    return fused(
         second_batch_tokens,
-        pre_expert_norm_scale,
-        group_router_columns,
-        expert_router_columns,
-        routes,
-        expert_gate_weight,
-        expert_up_weight,
-        expert_down_weight,
-    )
-    return (mixer_out, experts_out)
+        pre_expert_norm_scale.reshape(1, -1),
+        group_router_columns.T,
+        expert_router_columns.T,
+        routes.T,
+        expert_gate_weight[0],
+        expert_up_weight[0],
+        expert_down_weight[0],
+        mixed,
+        mixer_output_weight,
+    )
 
 
 def solution(mesh):

time: 238 us -> 150 us (0.63)
  waiting for transfers between devices: 106 us -> 7.8 us
  Pallas kernels: 0 us -> 81.8 us
  local copies, waits for them, and re-layouts: 39.6 us -> 21.2 us
  blocking collectives: 14.9 us -> 0 us
  matrix products: 26.3 us -> 12.3 us
  between operations: 14.5 us -> 1.05 us
  starting transfers between devices: 16 us -> 10.6 us
  other arithmetic: 17 us -> 12.4 us
    pallas_call x0 -> x1, Pallas kernels: none -> 81.8 us  [fused(): pl.pallas_call(kernel, out_shape=(jax.ShapeDtypeStruct((128, 2048), bf16)...]
    reduce_scatter x1 -> x0, waiting for transfers between devices: 53.5 us -> none  [mixer_half(): lax.psum_scatter(jnp.dot(mixed, mixer_output_weight, preferred_element_ty...]
    all_gather x1 -> x0, waiting for transfers between devices: 35.5 us -> none  [expert_half(): rows = lax.all_gather(arrived, 'tp', axis=1, tiled=True)]
    unnamed x54 -> x36, local copies, waits for them, and re-layouts: 19.1 us -> 3.78 us
    all_to_all x1 -> x0, blocking collectives: 14.9 us -> none  [expert_half(): lax.all_to_all(own_share, 'ep', split_axis=0, concat_axis=0, tiled=True)]
    dot_general x6 -> x0, matrix products: 14.7 us -> none  [the longest x1 5.6 us: mixer_half(): jnp.dot(mixed, mixer_output_weight, preferred_element_type=jnp.float32)]
    all_to_all x1 -> x0, waiting for transfers between devices: 7.18 us -> none  [expert_half(): lax.all_to_all(going_back, 'ep', split_axis=1, concat_axis=1, tiled=True)]
    gather x2 -> x0, local copies, waits for them, and re-layouts: 7.06 us -> none  [the longest x1 6.02 us: expert_half(): jnp.take(padded, source, axis=0)]
  transfers between devices with their start and end apart: 6 -> 2, of which waited for: 5 -> 1; matrix products, arithmetic and copies ran while one was open for 27% -> 5% of each run, Pallas kernels for 0% -> 0%
where the time goes in v1:
time: 150 us; the launch traced here: 147 us
  Pallas kernels  81.8 us (55%)
  local copies, waits for them, and re-layouts  21.2 us (14%)
  other arithmetic  12.4 us (8%)
  matrix products  12.3 us (8%)
  starting transfers between devices  10.6 us (7%)
  waiting for transfers between devices  7.8 us (5%)
    pallas_call x1, Pallas kernels, fused(): pl.pallas_call(kernel, out_shape=(jax.ShapeDtypeStruct((128, 2048), bf16)...  81.8 us
    all_to_all x1, waiting for transfers between devices, from_everyone(): lax.all_to_all(jnp.broadcast_to(value[None], (size, *value.shape)), axis,...  7.8 us
    all_to_all x1, starting transfers between devices, from_everyone(): lax.all_to_all(jnp.broadcast_to(value[None], (size, *value.shape)), axis,...  6.53 us
    reshape x2, local copies, waits for them, and re-layouts, mixer_half(): ssm = (inner + carried).reshape(length, heads_dev, head_dim)  5.61 us
    dot_general x1, matrix products, mixer_half(): jnp.einsum('bls,hbls,bshp->blhp', scores, weight, x_dt, precision=exact_p...  4.57 us
    ppermute x1, starting transfers between devices, from_behind(): lax.ppermute(value, axis, [(source, source + steps) for source in range(f...  4.05 us
    unnamed x36, local copies, waits for them, and re-layouts  3.78 us
  transfers between devices with their start and end apart: 2, of which 1 were waited for; matrix products, arithmetic and copies ran while one was open for 5% of the time, Pallas kernels for 0%

profile of v1, /device:TPU:1, one launch (start us, length us, event | category | flops | bytes accessed | tf_op | source)
XLA Modules:
  0.0 147.1 jit_solution(2996483398492815543)
XLA Ops:
  0.7 1.6 %constant_dynamic-slice_fusion = (bf16[2048,64]{1,0:T(8,128)(2,1)S(1)}, bf16[2048,64]{1,0:T(8,128)(2,1)S(1)}) fusion(bf16[2048,256]{1,0:T(8,128)(2,1)} %param.24, s32[]{:T(128)S(6)} %select_n.43, bf16[2048,256]{1,0:T(8,128)(2,1)} %param.23), kind=kLoop, calls=%fused_computation.86 | loop fusion | bytes 1048580 | tf_op jit(solution)/shard_map/dynamic_slice | solution.py:423
  2.5 4.1 %collective-permute-start = (bf16[3,256]{1,0:T(4,128)(2,1)S(1)}, bf16[3,256]{1,0:T(4,128)(2,1)S(1)}, u32[]{:S(2)}, u32[]{:S(2)}) collective-permute-start(bf16[3,256]{1,0:T(4,128)(2,1)S(1)} %pad_maximum_fusion.1), channel_id=1, source_target_pairs={{0,16},{16,32},{32,48},{48,64},{64,80},{80,96},{96,112},{112,128},... | collective-permute-start | bytes 4616 | tf_op jit(solution)/shard_map/ppermute | solution.py:335
  6.7 0.6 reduce_window_sum.24
  7.2 0.2 slice_reduce_fusion
  7.5 0.2 reduce_window_sum.25
  7.7 0.2 slice_reduce_fusion.1
  8.0 0.1 constant_dynamic-slice_fusion.2
  8.2 0.1 copy.85
  8.3 0.2 subtract_reduce_fusion
  8.4 0.3 convert_multiply_fusion
  8.8 0.1 copy.87
  8.9 1.3 copy.97
  10.3 0.1 mul.235
  10.4 0.6 reshape.85.nsc
  11.0 0.5 maximum_convert_fusion
  11.5 1.3 multiply_convert_fusion
  12.8 1.2 fusion.47
  14.0 0.3 copy.81
  14.4 0.2 copy.116
  14.6 1.1 broadcast_multiply_fusion
  15.7 0.9 fusion.23
  16.6 1.2 fusion.31
  17.8 0.1 copy.104
  17.9 0.1 reshape.91
  18.0 0.8 broadcast_in_dim.84
  18.9 6.5 %all-to-all-start = ((bf16[16,129,64]{1,2,0:T(8,128)(2,1)}), bf16[16,129,64]{1,2,0:T(8,128)(2,1)}, u32[]{:S(2)}, u32[]{:S(2)}) async-start(bf16[16,129,64]{1,2,0:T(8,128)(2,1)} %broadcast_in_dim.84), calls=%async_computation | async-start | bytes 1048576 | tf_op jit(solution)/shard_map/all_to_all | solution.py:340
  25.4 2.7 %fusion.48 = f32[16,128,128]{2,1,0:T(8,128)} fusion(bf16[16,128,64]{2,1,0:T(8,128)(2,1)} %bitcast.93, bf16[16,128,64]{2,1,0:T(8,128)(2,1)} %bitcast.95), kind=kOutput, calls=%fused_computation.98 | convolution fusion | flops 33554432 | bytes 1572864 | tf_op jit(solution)/shard_map/bln,bsn->bls/dot_general | solution.py:443
  28.1 7.8 %all-to-all-done = bf16[16,129,64]{1,2,0:T(8,128)(2,1)} async-done(((bf16[16,129,64]{1,2,0:T(8,128)(2,1)}), bf16[16,129,64]{1,2,0:T(8,128)(2,1)}, u32[]{:S(2)}, u32[]{:S(2)}) %all-to-all-start) | async-done | bytes 264224 | tf_op jit(solution)/shard_map/all_to_all | solution.py:340
  35.9 1.0 slice.145
  36.8 0.2 copy.113
  37.2 1.8 %slice_convert_fusion.1 = f32[16,128,64]{1,2,0:T(8,128)} fusion(bf16[16,129,64]{1,2,0:T(8,128)(2,1)} %all-to-all-done), kind=kLoop, calls=%fused_computation.47 | loop fusion | flops 131072 | bytes 786432 | tf_op jit(solution)/shard_map/convert_element_type | solution.py:377
  39.1 2.4 %copy.110 = f32[16,128,64]{2,1,0:T(8,128)} copy(f32[16,128,64]{1,2,0:T(8,128)} %slice_convert_fusion.1) | data formatting | bytes 1048576 | tf_op jit(solution)/shard_map/convert_element_type | solution.py:377
  41.4 1.4 broadcast_select_fusion
  42.8 0.1 slice_add_fusion
  42.9 0.1 slice_add_fusion.1
  43.0 0.1 slice_add_fusion.2
  43.2 1.6 %fusion.15 = f32[16,2,64,64]{3,0,2,1:T(8,128)S(1)} fusion(f32[16,2,64,64]{3,2,1,0:T(8,128)S(1)} %fusion.23, f32[2,64,64]{2,1,0:T(8,128)S(1)} %fusion.34, f32[16,2]{0,1:T(2,128)S(1)} %get-tuple-element.14, f32[2,16]{1,0:T(2,128)S(1)} %reduce_window_sum.25, f32[2,16]{1,0:T(2,128)S(1)} %subtract_reduce_fusion, pred[16,16]{1,0:T(8,128)(4,1)S(1)} %iota_compare_fusion.1), kind=kOutput, calls=%fused_computation.18 | convolution fusion | flops 25429504 | bytes 1081984 | tf_op jit(solution)/shard_map/hbc,chpn->bhpn/dot_general | solution.py:464
  44.9 1.3 convolution_multiply_fusion
  46.2 4.6 %fusion.12 = f32[16,128,2,64]{1,3,2,0:T(8,128)S(1)} fusion(f32[16,128,2,64]{1,3,2,0:T(8,128)S(1)} %convolution_multiply_fusion, f32[16,128,2,64]{1,0,3,2:T(8,128)S(1)} %copy-done.5, f32[16,128,128]{2,1,0:T(8,128)S(1)} %copy-done.6, f32[2,16,128]{2,0,1:T(2,128)S(1)} %copy.77, pred[128,128]{1,0:T(8,128)(4,1)S(1)} %iota_compare_fusion), kind=kOutput, calls=%fused_computation.15 | convolution fusion | flops 405012480 | bytes 4227072 | tf_op jit(solution)/shard_map/bls,hbls,bshp->blhp/dot_general | solution.py:444
  50.8 2.3 %copy.111 = f32[16,128,2,64]{3,2,1,0:T(2,128)} copy(f32[16,128,2,64]{1,3,2,0:T(8,128)S(1)} %fusion.12) | data formatting | bytes 2097152 | tf_op jit(solution)/shard_map/reshape | solution.py:468
  53.1 3.3 %reshape.108 = f32[2048,128]{1,0:T(8,128)} reshape(f32[16,128,2,64]{3,2,1,0:T(2,128)} %copy.111) | data formatting | bytes 2097152 | tf_op jit(solution)/shard_map/reshape | solution.py:468
  56.4 1.5 %fusion.21 = f32[2048,2]{0,1:T(2,128)S(1)} fusion(f32[2]{0:T(128)S(1)} %copy-done.13, f32[2048,128]{0,1:T(8,128)} %copy.97, f32[2048,128]{0,1:T(8,128)S(1)} %copy.81, f32[16,128,2,64]{1,3,2,0:T(8,128)S(1)} %fusion.12), kind=kLoop, calls=%fused_computation.28 | loop fusion | flops 1306624 | bytes 3162120 | tf_op jit(solution)/shard_map/reduce_sum | solution.py:472
  58.0 0.1 mul.244
  58.1 1.3 copy.98
  59.4 2.6 %multiply_convert_fusion.1.mixed_h = bf16[2048,128]{1,0:T(8,128)(2,1)} fusion(f32[2048,128]{1,0:T(8,128)} %copy.98, f32[2048,128]{1,0:T(8,128)S(1)} %copy-done.2, f32[128]{0:T(128)S(1)} %convert_element_type.54, f32[128]{0:T(128)S(1)} %mul.235, bf16[2048,256]{1,0:T(8,128)(2,1)S(1)} %multiply_convert_fusion, bf16[2048,128]{1,0:T(8,128)(2,1)} %param.22), kind=kLoop, calls=%fused_computation.33 | loop fusion | flops 3145728 | bytes 3671040 | tf_op jit(solution)/shard_map/convert_element_type | solution.py:473
  62.0 81.8 %shard_map.212 = (bf16[128,2048]{1,0:T(8,128)(2,1)}, bf16[256,128]{1,0:T(8,128)(2,1)}) custom-call(bf16[256,2048]{1,0:T(8,128)(2,1)} %tok.1, bf16[1,2048]{1,0:T(2,128)(2,1)} %reshape.85.nsc, bf16[4,2048]{1,0:T(4,128)(2,1)} %bitcast.105, bf16[16,2048]{1,0:T(8,128)(2,1)} %bitcast.104, s32[2,256]{1,0:T(2,128)} %bitcast.113, bf16[2048,256]{1,0:T(8,128)(2,1)} %bitcast.100, ...), custom_call_target="tpu_custom_call" | custom-call | tf_op jit(solution)/shard_map/pallas_call | solution.py:296
  143.8 1.9 %copy.133 = bf16[128,2048]{1,0:T(8,128)(2,1)} copy(bf16[128,2048]{1,0:T(8,128)(2,1)} %get-tuple-element.24) | data formatting | bytes 1048576
  145.7 1.5 %copy.134 = bf16[256,128]{1,0:T(8,128)(2,1)} copy(bf16[256,128]{1,0:T(8,128)(2,1)} %get-tuple-element.25) | data formatting | bytes 131072
  (65 shorter events, 1.0 us)
Async XLA Ops:
  0.6 1.7 %copy-start.3 = (bf16[2048,128]{1,0:T(8,128)(2,1)S(1)}, bf16[2048,128]{1,0:T(8,128)(2,1)}, u32[]{:S(2)}) copy-start(bf16[2048,128]{1,0:T(8,128)(2,1)} %param.21) | copy-start | bytes 1572868
  0.6 5.9 %copy-start.14 = (f32[2]{0:T(128)S(1)}, f32[2]{0:T(128)}, u32[]{:S(2)}) copy-start(f32[2]{0:T(128)} %param.29) | copy-start | bytes 28
  0.7 5.9 %copy-start.7 = (f32[2,2048]{1,0:T(2,128)S(1)}, f32[2,2048]{1,0:T(2,128)}, u32[]{:S(2)}) copy-start(f32[2,2048]{1,0:T(2,128)} %param.28) | copy-start | bytes 49156
  0.7 5.9 %copy-start.8 = (f32[2,2048]{1,0:T(2,128)S(1)}, f32[2,2048]{1,0:T(2,128)}, u32[]{:S(2)}) copy-start(f32[2,2048]{1,0:T(2,128)} %param.30) | copy-start | bytes 49156
  0.7 7.3 %copy-start.12 = (bf16[4,256]{1,0:T(4,128)(2,1)S(1)}, bf16[4,256]{1,0:T(4,128)(2,1)}, u32[]{:S(2)}) copy-start(bf16[4,256]{1,0:T(4,128)(2,1)} %param.26) | copy-start | bytes 6148
  0.7 7.3 %copy-start.11 = (bf16[4,256]{1,0:T(4,128)(2,1)S(1)}, bf16[4,256]{1,0:T(4,128)(2,1)}, u32[]{:S(2)}) copy-start(bf16[4,256]{1,0:T(4,128)(2,1)} %param.27) | copy-start | bytes 6148
  0.7 7.4 %copy-start.10 = (bf16[4,128]{1,0:T(4,128)(2,1)S(1)}, bf16[4,128]{1,0:T(4,128)(2,1)}, u32[]{:S(2)}) copy-start(bf16[4,128]{1,0:T(4,128)(2,1)} %param.25) | copy-start | bytes 3076
  0.7 7.7 %copy-start.4 = (bf16[2048,128]{1,0:T(8,128)(2,1)S(1)}, bf16[2048,128]{1,0:T(8,128)(2,1)}, u32[]{:S(2)}) copy-start(bf16[2048,128]{1,0:T(8,128)(2,1)} %param.22) | copy-start | bytes 1572868
  2.5 7.8 %copy-start.13 = (f32[2]{0:T(128)S(1)}, f32[2]{0:T(128)}, u32[]{:S(2)}) copy-start(f32[2]{0:T(128)} %param.31) | copy-start | bytes 28
  2.5 7.9 %copy-start.15 = (bf16[128]{0:T(256)(128)(2,1)S(1)}, bf16[128]{0:T(256)(128)(2,1)}, u32[]{:S(2)}) copy-start(bf16[128]{0:T(256)(128)(2,1)} %param.32) | copy-start | bytes 772
  2.5 7.9 %copy-start.9 = (bf16[2048]{0:T(1024)(128)(2,1)S(1)}, bf16[2048]{0:T(1024)(128)(2,1)}, u32[]{:S(2)}) copy-start(bf16[2048]{0:T(1024)(128)(2,1)} %param.35) | copy-start | bytes 12292
  2.5 8.5 %collective-permute-start = (bf16[3,256]{1,0:T(4,128)(2,1)S(1)}, bf16[3,256]{1,0:T(4,128)(2,1)S(1)}, u32[]{:S(2)}, u32[]{:S(2)}) collective-permute-start(bf16[3,256]{1,0:T(4,128)(2,1)S(1)} %pad_maximum_fusion.1), channel_id=1, source_target_pairs={{0,16},{16,32},{32,48},{48,64},{64,80},{80,96},{96,112},{112,128},... | collective-permute-start | bytes 4616 | tf_op jit(solution)/shard_map/ppermute | solution.py:335
  14.6 1.1 copy-start.1
  18.9 17.0 %all-to-all-start = ((bf16[16,129,64]{1,2,0:T(8,128)(2,1)}), bf16[16,129,64]{1,2,0:T(8,128)(2,1)}, u32[]{:S(2)}, u32[]{:S(2)}) async-start(bf16[16,129,64]{1,2,0:T(8,128)(2,1)} %broadcast_in_dim.84), calls=%async_computation | async-start | bytes 1048576 | tf_op jit(solution)/shard_map/all_to_all | solution.py:340
  42.9 1.9 %copy-start = (bf16[2048,64]{1,0:T(8,128)(2,1)S(1)}, bf16[2048,64]{1,0:T(8,128)(2,1)}, u32[]{:S(2)}) copy-start(bf16[2048,64]{1,0:T(8,128)(2,1)} %get-tuple-element.5) | copy-start | bytes 786436
  43.2 3.0 %copy-start.5 = (f32[16,128,2,64]{1,0,3,2:T(8,128)S(1)}, f32[16,128,2,64]{1,0,3,2:T(8,128)}, u32[]{:S(2)}) copy-start(f32[16,128,2,64]{1,0,3,2:T(8,128)} %get-tuple-element.3) | copy-start | bytes 3145732
  43.2 3.0 %copy-start.6 = (f32[16,128,128]{2,1,0:T(8,128)S(1)}, f32[16,128,128]{2,1,0:T(8,128)}, u32[]{:S(2)}) copy-start(f32[16,128,128]{2,1,0:T(8,128)} %fusion.48) | copy-start | bytes 3145732
  57.9 1.4 copy-start.2

commit v2 on v1

v2 whole, which is shorter than its diff:
```python
import jax
import jax.numpy as jnp
from jax import lax
from jax.experimental import pallas as pl
from jax.experimental.pallas import tpu as pltpu
from jax.sharding import PartitionSpec as P

eps = 1e-06
exact_prec = lax.Precision.HIGHEST
bf16, f32 = jnp.bfloat16, jnp.float32

NEP = 16
NZ = 8
CAP = 64
HALF = CAP // 2
ORDER = (4, 3, 5, 2, 6, 1, 7, 0)


def kernel(
    tok, nsc, rg, re, rt, ut, bt, ct, sl, ex, gn, rate, direct,
    gate_h, up_h, down_h, w_h, u_h, og_h, bm_h, cm_h,
    mo, eo,
    nrm, sbuf, xr, gw, uw, dn, hall, ysend, ybuf, zsend, zbuf, wg, mx, psend, precv,
    ub, bb, cb, ogb, xsb, csb, c0l, c1l, dtl, cumr, dtr, tst, ssm, spad, ssend, sst, entb, mixb,
    loc_s, dnl_s, dns_s, dnr_s, xs_s, xr_s, xf_s, xg_s, hs_s, hr_s, ys_s, yr_s, zs_s, zr_s,
    ws_s, wr_s, ms_s, mr_s, fs_s, fr_s, hl_s, hh_s, ss_s, sr_s,
):
    ep, tp = lax.axis_index("ep"), lax.axis_index("tp")
    y, x = ep // 4, ep % 4
    z, c = tp // 2, tp % 2
    other = z * 2 + (1 - c)

    def ep_at(d, sign):
        return ((y + 4 + sign * (d // 4)) % 4) * 4 + (x + 4 + sign * (d % 4)) % 4

    def tp_at(r):
        return ((z + r) % NZ) * 2 + c

    def push(src, dst, ss, rs, e, t):
        return pltpu.make_async_remote_copy(
            src_ref=src, dst_ref=dst, send_sem=ss, recv_sem=rs,
            device_id={"ep": e, "tp": t}, device_id_type=pl.DeviceIdType.MESH,
        )

    barrier = pltpu.get_barrier_semaphore()

    def greet(e, t):
        pl.semaphore_signal(
            barrier, inc=1, device_id={"ep": e, "tp": t}, device_id_type=pl.DeviceIdType.MESH
        )

    lg = pltpu.make_async_copy(gate_h, gw, loc_s.at[0])
    lu = pltpu.make_async_copy(up_h, uw, loc_s.at[1])
    lw = pltpu.make_async_copy(w_h, wg.at[pl.ds(0, 128), :], loc_s.at[2])
    grp = tp // 4
    map_cols = pl.ds(pl.multiple_of((grp // 2) * 128, 128), 128)
    body, tail = pl.ds(8, 2048), pl.ds(2040, 8)
    l_mix = [
        pltpu.make_async_copy(u_h, ub.at[body, :], loc_s.at[4]),
        pltpu.make_async_copy(bm_h.at[:, map_cols], bb.at[body, :], loc_s.at[5]),
        pltpu.make_async_copy(cm_h.at[:, map_cols], cb.at[body, :], loc_s.at[6]),
        pltpu.make_async_copy(og_h, ogb, loc_s.at[3]),
    ]
    for cp in l_mix + [lg, lu, lw]:
        cp.start()

    def down_cols(q, core):
        return down_h.at[:, pl.ds(pl.multiple_of((2 * ((z + ORDER[q]) % NZ) + core) * 128, 128), 128)]

    dn_l = [
        pltpu.make_async_copy(
            down_cols(q, c), dn.at[c, :, pl.ds(q * 128, 128)], dnl_s.at[q]
        )
        for q in range(NZ)
    ]
    for cp in dn_l:
        cp.start()

    for d in range(1, NEP):
        greet(ep_at(d, 1), tp)
    for r in range(1, NZ):
        greet(ep, tp_at(r))
    greet(ep, other)
    def norm_rows(i, _):
        rows = pl.ds(pl.multiple_of(i * 32, 32), 32)
        v = tok[rows, :].astype(f32)
        v = v * lax.rsqrt(jnp.mean(v * v, axis=1, keepdims=True) + eps) * nsc[...].astype(f32)
        nrm[rows, :] = v.astype(bf16)
        return 0

    lax.fori_loop(0, 8, norm_rows, 0)

    r0, r1 = rt[0:1, :], rt[1:2, :]
    di = lax.broadcasted_iota(jnp.int32, (NEP, 256), 0)
    e_rel = (((y + lax.shift_right_logical(di, 2)) & 3) * 4) + ((x + di) & 3)
    in0, in1 = e_rel == r0, e_rel == r1
    routed = in0 | in1
    onehot = jnp.where(routed, 1.0, 0.0).astype(bf16)
    a = lax.broadcasted_iota(jnp.int32, (256, 256), 0)
    b = lax.broadcasted_iota(jnp.int32, (256, 256), 1)
    before = jnp.where(a < b, 1.0, 0.0).astype(bf16)
    place = jnp.dot(onehot, before, preferred_element_type=f32)
    place = jnp.where(routed, place, -1.0)
    slot = lax.broadcasted_iota(jnp.int32, (HALF, 256), 0) + HALF * c
    slot = slot.astype(f32)
    tokens_n = nrm[...]
    for q in range(4):
        pick = jnp.concatenate(
            [jnp.where(place[d : d + 1, :] == slot, 1.0, 0.0) for d in range(4 * q, 4 * q + 4)], axis=0
        ).astype(bf16)
        sbuf[q * 128 : (q + 1) * 128, :] = jnp.dot(pick, tokens_n, preferred_element_type=f32).astype(bf16)
    pl.semaphore_wait(barrier, NEP - 1 + NZ - 1 + 1)
    after = (ep + 1) % NEP
    halo = [
        push(u_h.at[tail, :], ub.at[pl.ds(0, 8), :], hl_s.at[0], hh_s.at[0], after, tp),
        push(bm_h.at[tail, map_cols], bb.at[pl.ds(0, 8), :], hl_s.at[1], hh_s.at[1], after, tp),
        push(cm_h.at[tail, map_cols], cb.at[pl.ds(0, 8), :], hl_s.at[2], hh_s.at[2], after, tp),
    ]
    for cp in halo:
        cp.start()

    dn_r = [
        push(down_cols(q, 1 - c), dn.at[c, :, pl.ds(q * 128, 128)], dns_s.at[q], dnr_s.at[q], ep, other)
        for q in range(NZ)
    ]
    for cp in dn_r:
        cp.start()
    def w_copy(way, k):
        if way == 0:
            a, b, t = (9 - k) % NZ, NZ - k, tp_at(1)
        else:
            a, b, t = k - 1, k, tp_at(NZ - 1)
        lo, n = (0, 128) if k < 4 else (64 * way, 64)
        src = w_h.at[pl.ds(lo, n), :] if k == 1 else wg.at[pl.ds(a * 128 + lo, n), :]
        return push(
            src, wg.at[pl.ds(b * 128 + lo, n), :], ws_s.at[way, k - 1], wr_s.at[way, k - 1], ep, t
        )

    w_cp = [[w_copy(way, k) for k in range(1, 5)] for way in range(2)]

    def w_step(k):
        for way in range(2):
            if k > 1:
                w_cp[way][k - 2].wait_recv()
            w_cp[way][k - 1].start()

    w_step(1)

    x_cp = [
        push(
            sbuf.at[pl.ds(d * HALF, HALF), :],
            xr.at[pl.ds(pl.multiple_of(d * CAP + HALF * c, HALF), HALF), :],
            xs_s.at[d], xr_s.at[d], ep_at(d, 1), tp,
        )
        for d in range(1, NEP)
    ]
    for cp in x_cp[:7]:
        cp.start()
    xr[pl.ds(pl.multiple_of(HALF * c, HALF), HALF), :] = sbuf[0:HALF, :]

    nt = (((1,), (1,)), ((), ()))
    gl = lax.dot_general(rg[...], tokens_n, nt, preferred_element_type=f32)
    el = lax.dot_general(re[...], tokens_n, nt, preferred_element_type=f32)

    def lse(v):
        top = jnp.max(v, axis=0, keepdims=True)
        return top + jnp.log(jnp.sum(jnp.exp(v - top), axis=0, keepdims=True))

    gl = gl - lse(gl)
    ei = lax.broadcasted_iota(jnp.int32, (4, 256), 0)
    lp0 = jnp.zeros((1, 256), f32)
    lp1 = jnp.zeros((1, 256), f32)
    for g in range(4):
        part = el[4 * g : 4 * g + 4, :]
        part = part - lse(part) + gl[g : g + 1, :]
        lp0 += jnp.sum(jnp.where(ei + 4 * g == r0, part, 0.0), axis=0, keepdims=True)
        lp1 += jnp.sum(jnp.where(ei + 4 * g == r1, part, 0.0), axis=0, keepdims=True)
    top = jnp.maximum(lp0, lp1)
    w0, w1 = jnp.exp(lp0 - top), jnp.exp(lp1 - top)
    total = w0 + w1
    share = jnp.where(in0, w0 / total, 0.0) + jnp.where(in1, w1 / total, 0.0)
    both = jnp.concatenate([place, share, jnp.zeros((96, 256), f32)], axis=0).T

    lane = lax.broadcasted_iota(jnp.int32, (256, 128), 1)
    in_slot = (lane & (CAP - 1)).astype(f32)
    low = lane < CAP
    mixw = []
    for p in range(8):
        at = jnp.where(low, both[:, 2 * p : 2 * p + 1], both[:, 2 * p + 1 : 2 * p + 2])
        sh = jnp.where(low, both[:, 16 + 2 * p : 17 + 2 * p], both[:, 17 + 2 * p : 18 + 2 * p])
        mixw.append(jnp.where(at == in_slot, sh, 0.0).astype(bf16))
    mixw = jnp.concatenate(mixw, axis=1)

    row = lax.broadcasted_iota(jnp.int32, (32, 128), 0)
    lane1 = lax.broadcasted_iota(jnp.int32, (1, 128), 1)
    first = lax.broadcasted_iota(jnp.int32, (128, 128), 1) < 64
    at_l = lax.broadcasted_iota(jnp.int32, (128, 128), 0)
    at_s = lax.broadcasted_iota(jnp.int32, (128, 128), 1)
    lower = at_l >= at_s
    sv = sl[...]
    dt = jnp.maximum(sv, 0.0) + jnp.log1p(jnp.exp(-jnp.abs(sv)))
    speed = jnp.exp(jnp.where((row & 1) == 0, rate[0], rate[1]))
    log_decay = ex[...] - dt * speed
    upto = jnp.where(at_l <= at_s, 1.0, 0.0).astype(f32)
    cum = jnp.dot(log_decay, upto, precision=exact_prec, preferred_element_type=f32)
    cumr[...] = cum
    dtr[...] = dt
    turned = jnp.concatenate([cum, dt, jnp.zeros((64, 128), f32)], axis=0).T
    for b in range(16):
        rows = slice(128 * b, 128 * (b + 1))
        c0l[rows, :] = jnp.broadcast_to(turned[:, 2 * b : 2 * b + 1], (128, 128))
        c1l[rows, :] = jnp.broadcast_to(turned[:, 2 * b + 1 : 2 * b + 2], (128, 128))
        dtl[rows, :] = jnp.where(first, turned[:, 32 + 2 * b : 33 + 2 * b], turned[:, 33 + 2 * b : 34 + 2 * b])

    for cp in l_mix:
        cp.wait()
    for cp in halo:
        cp.wait_recv()
    for buf in (ub, bb, cb):
        edge = buf[0:8, :]
        buf[0:8, :] = jnp.where(ep == 0, jnp.zeros_like(edge), edge)
    tap_u = ut[...].astype(f32)
    block_0 = grp // 2 == 0
    tap_b = jnp.where(block_0, bt[:, 0:128].astype(f32), bt[:, 128:256].astype(f32))
    tap_c = jnp.where(block_0, ct[:, 0:128].astype(f32), ct[:, 128:256].astype(f32))
    own_half = (lane1 // 64) == grp % 2

    def conv(buf, taps, base):
        ext = buf[pl.ds(base, 136), :].astype(f32)
        tot = taps[0:1, :] * ext[5:133, :]
        for j in range(1, 4):
            tot += taps[j : j + 1, :] * ext[5 + j : 133 + j, :]
        return tot * jax.nn.sigmoid(tot)

    def one_block(b, carry):
        state, since = carry
        base = pl.multiple_of(b * 128, 128)
        rows = pl.ds(base, 128)
        xs = conv(ub, tap_u, base).astype(bf16)
        bs = conv(bb, tap_b, base).astype(bf16)
        cs = jnp.where(own_half, conv(cb, tap_c, base), 0.0).astype(bf16)
        xsb[rows, :] = xs
        csb[rows, :] = cs
        tst[pl.ds(b, 1), :] = since
        scores = lax.dot_general(cs, bs, (((1,), (1,)), ((), ())), preferred_element_type=f32)
        inner = []
        for h, col in ((0, c0l), (1, c1l)):
            at = pl.ds(2 * b + h, 1)
            diff = jnp.where(lower, col[rows, :] - cumr[at, :], 0.0)
            near = jnp.where(lower, scores * jnp.exp(diff) * dtr[at, :], 0.0).astype(bf16)
            inner.append(jnp.dot(near, xs, preferred_element_type=f32))
        both_cum = jnp.where(first, c0l[rows, :], c1l[rows, :])
        carried = jnp.dot(cs, state.astype(bf16), preferred_element_type=f32) * jnp.exp(both_cum)
        ssm[rows, :] = jnp.where(first, inner[0], inner[1]) + carried
        last = both_cum[127:128, :]
        weighed = (xs.astype(f32) * (jnp.exp(last - both_cum) * dtl[rows, :])).astype(bf16)
        gained = lax.dot_general(bs, weighed, (((0,), (0,)), ((), ())), preferred_element_type=f32)
        return state * jnp.exp(last) + gained, since + last

    state, since = lax.fori_loop(
        0, 16, one_block, (jnp.zeros((128, 128), f32), jnp.zeros((1, 128), f32))
    )
    spad[...] = state
    half_rows = pl.ds(pl.multiple_of((grp % 2) * 64, 64), 64)
    ssend[0:64, :] = spad[half_rows, :].astype(bf16)
    decay = jnp.exp(since)
    near_decay = decay.astype(bf16)
    rest_decay = (decay - near_decay.astype(f32)).astype(bf16)
    row8 = lax.broadcasted_iota(jnp.int32, (8, 128), 0)
    ssend[64:72, :] = jnp.where(
        row8 == 0, near_decay.astype(f32), jnp.where(row8 == 1, rest_decay.astype(f32), 0.0)
    ).astype(bf16)
    s_cp = [
        push(ssend, sst.at[ep], ss_s.at[d], sr_s.at[d], ep_at(d, 1), tp) for d in range(1, NEP)
    ]
    for cp in s_cp:
        cp.start()
    for cp in x_cp[7:]:
        cp.start()
    w_step(2)


    def mixer_rest():
        for cp in s_cp:
            cp.wait_recv()

        def chain(j, ent):
            got = sst[j].astype(f32)
            return jnp.where(j < ep, ent * (got[64:65, :] + got[65:66, :]) + got[0:64, :], ent)

        ent = lax.fori_loop(0, NEP - 1, chain, jnp.zeros((64, 128), f32))
        entb[...] = jnp.zeros_like(entb)
        entb[half_rows, :] = ent.astype(bf16)
        scale = jnp.where(lane1 < 64, direct[0], direct[1])
        gain = gn[...].astype(f32)

        def rows_of(j, keep):
            for k in range(2):
                b = 2 * j + k
                rows = pl.ds(pl.multiple_of(b * 128, 128), 128)
                since_b = jnp.where(first, c0l[rows, :], c1l[rows, :]) + tst[pl.ds(b, 1), :]
                far = jnp.dot(csb[rows, :], entb[...], preferred_element_type=f32) * jnp.exp(since_b)
                gate = ogb[rows, :].astype(f32)
                val = (ssm[rows, :] + far + scale * xsb[rows, :].astype(f32)) * (gate * jax.nn.sigmoid(gate))
                sq = val * val
                sum0 = jnp.sum(jnp.where(first, sq, 0.0), axis=1, keepdims=True)
                sum1 = jnp.sum(jnp.where(first, 0.0, sq), axis=1, keepdims=True)
                ms = jnp.where(first, sum0, sum1) * (1.0 / 64)
                keep(k, rows, (val * lax.rsqrt(ms + eps) * gain).astype(bf16))

        def send_on(i, _):
            j = (z + 1 + i) % NZ

            def keep(k, rows, val):
                mixb[rows, :] = val

            rows_of(j, keep)
            push(
                mixb.at[pl.ds(pl.multiple_of(j * 256, 256), 256), :],
                mx.at[:, pl.ds(pl.multiple_of((7 - i) * 128, 128), 128)],
                ms_s.at[7 - i], mr_s.at[7 - i], ep, tp_at(1 + i),
            ).start()
            return 0

        lax.fori_loop(0, NZ - 1, send_on, 0)

        def own(k, rows, val):
            mx[128 * k : 128 * (k + 1), 0:128] = val

        rows_of(z, own)

    m_cp = [
        push(
            mixb.at[pl.ds(pl.multiple_of(((z + r) % NZ) * 256, 256), 256), :],
            mx.at[:, pl.ds((NZ - r) * 128, 128)],
            ms_s.at[NZ - r], mr_s.at[NZ - r], ep, tp_at(r),
        )
        for r in range(1, NZ)
    ]

    lg.wait()
    lu.wait()
    for cp in dn_l:
        cp.wait()

    def x_hand(d):
        rows = pl.ds(pl.multiple_of(d * CAP + HALF * c, HALF), HALF)
        return push(xr.at[rows, :], xr.at[rows, :], xf_s.at[d], xg_s.at[d], ep, other)

    hand = [x_hand(d) for d in range(NEP)]

    def y_copy(d, h):
        part = (pl.ds(d * CAP, CAP), pl.ds(h * 512, 512))
        return push(ysend.at[part], ybuf.at[part], ys_s.at[h, d], yr_s.at[h, d], ep_at(d, -1), tp)

    y_cp = [[y_copy(d, h) for d in range(1, NEP)] for h in range(2)]
    h_cp = []
    for g in range(4):
        for d in range(4 * g, 4 * g + 4):
            if d > 0:
                x_cp[d - 1].wait_recv()
            hand[d].start()
        for d in range(4 * g, 4 * g + 4):
            hand[d].wait_recv()
        rows = slice(256 * g, 256 * (g + 1))
        xg = xr[rows, :]
        gv = jnp.dot(xg, gw[...], preferred_element_type=f32)
        uv = jnp.dot(xg, uw[...], preferred_element_type=f32)
        hall[c, rows, :] = (gv * jax.nn.sigmoid(gv) * uv).astype(bf16)
        part = hall.at[c, pl.ds(256 * g, 256), :]
        cp = push(part, part, hs_s.at[g], hr_s.at[g], ep, other)
        cp.start()
        h_cp.append(cp)
        if g == 0:
            for cq in dn_r:
                cq.wait_recv()
        if g == 2:
            w_step(3)
            mixer_rest()
        cp.wait_recv()
        yv = jnp.dot(hall[0, rows, :], dn[0], preferred_element_type=f32)
        yv += jnp.dot(hall[1, rows, :], dn[1], preferred_element_type=f32)
        ysend[rows, :] = yv.astype(bf16)
        for d in range(4 * g, 4 * g + 4):
            if d > 0:
                y_cp[0][d - 1].start()
    for d in range(1, NEP):
        y_cp[1][d - 1].start()
    ybuf[0:CAP, :] = ysend[0:CAP, :]

    z_cp = []
    for h in range(2):
        for d in range(1, NEP):
            y_cp[h][d - 1].wait_recv()
        cols = slice(512 * h, 512 * (h + 1))
        comb = jnp.dot(mixw, ybuf[:, cols], preferred_element_type=f32)
        for i in range(4):
            r = ORDER[4 * h + i]
            val = comb[:, 128 * i : 128 * (i + 1)]
            if r == 0:
                zbuf[0] = val.astype(bf16)
                continue
            zsend[r] = val.astype(bf16)
            cp = push(zsend.at[r], zbuf.at[NZ - r], zs_s.at[NZ - r], zr_s.at[NZ - r], ep, tp_at(r))
            cp.start()
            z_cp.append(cp)
        if h == 0:
            w_step(4)

    lw.wait()
    for cp in m_cp:
        cp.wait_recv()
    for way in range(2):
        w_cp[way][3].wait_recv()
    theirs = mx[pl.ds(pl.multiple_of((1 - c) * 128, 128), 128), :]
    psend[...] = jnp.dot(theirs, wg[...], preferred_element_type=f32).astype(bf16)
    fin = push(psend, precv, fs_s, fr_s, ep, other)
    fin.start()
    ours = mx[pl.ds(pl.multiple_of(c * 128, 128), 128), :]
    mine = jnp.dot(ours, wg[...], preferred_element_type=f32)
    fin.wait_recv()
    mo[...] = (mine + precv[...].astype(f32)).astype(bf16)

    acc = zbuf[0].astype(f32)
    for cp in z_cp:
        cp.wait_recv()
    for r in range(1, NZ):
        acc += zbuf[r].astype(f32)
    eo[...] = acc.astype(bf16)

    for cp in dn_r + m_cp + x_cp + halo + s_cp + hand + y_cp[0] + y_cp[1] + h_cp + z_cp + [fin]:
        cp.wait_send()
    for way in range(2):
        for cp in w_cp[way]:
            cp.wait_send()


def fused(*args):
    vmem, hbm = pl.BlockSpec(memory_space=pltpu.VMEM), pl.BlockSpec(memory_space=pl.ANY)
    smem = pl.BlockSpec(memory_space=pltpu.SMEM)
    dma = pltpu.SemaphoreType.DMA
    v = pltpu.VMEM
    return pl.pallas_call(
        kernel,
        out_shape=(
            jax.ShapeDtypeStruct((128, 2048), bf16),
            jax.ShapeDtypeStruct((256, 128), bf16),
        ),
        in_specs=[vmem] * 11 + [smem] * 2 + [hbm] * 8,
        out_specs=(vmem, vmem),
        scratch_shapes=[
            v((256, 2048), bf16),
            v((512, 2048), bf16),
            v((1024, 2048), bf16),
            v((2048, 256), bf16),
            v((2048, 256), bf16),
            v((2, 256, 1024), bf16),
            v((2, 1024, 256), bf16),
            v((1024, 1024), bf16),
            v((1024, 1024), bf16),
            v((8, 256, 128), bf16),
            v((8, 256, 128), bf16),
            v((1024, 2048), bf16),
            v((256, 1024), bf16),
            v((128, 2048), bf16),
            v((128, 2048), bf16),
            v((2056, 128), bf16),
            v((2056, 128), bf16),
            v((2056, 128), bf16),
            v((2048, 128), bf16),
            v((2048, 128), bf16),
            v((2048, 128), bf16),
            v((2048, 128), f32),
            v((2048, 128), f32),
            v((2048, 128), f32),
            v((32, 128), f32),
            v((32, 128), f32),
            v((16, 128), f32),
            v((2048, 128), f32),
            v((128, 128), f32),
            v((72, 128), bf16),
            v((16, 72, 128), bf16),
            v((128, 128), bf16),
            v((2048, 128), bf16),
            dma((7,)), dma((8,)), dma((8,)), dma((8,)),
            dma((16,)), dma((16,)), dma((16,)), dma((16,)),
            dma((4,)), dma((4,)), dma((2, 16)), dma((2, 16)),
            dma((8,)), dma((8,)), dma((2, 4)), dma((2, 4)), dma((8,)), dma((8,)),
            dma, dma, dma((3,)), dma((3,)), dma((16,)), dma((16,)),
        ],
        compiler_params=pltpu.CompilerParams(
            collective_id=0, has_side_effects=True, vmem_limit_bytes=56 * 1024 * 1024
        ),
    )(*args)


def per_device(
    mixer_input_channels,
    output_gate_logits,
    head_group_input_map,
    head_group_output_map,
    input_channel_taps,
    input_map_taps,
    output_map_taps,
    step_logits,
    head_log_rate,
    extra_log_decay,
    head_direct_scale,
    gated_norm_scale,
    mixer_output_weight,
    second_batch_tokens,
    pre_expert_norm_scale,
    group_router_columns,
    expert_router_columns,
    routes,
    expert_gate_weight,
    expert_up_weight,
    expert_down_weight,
):
    def by_block(v):
        return jnp.transpose(v.reshape(2, 16, 128), (1, 0, 2)).reshape(32, 128)

    return fused(
        second_batch_tokens,
        pre_expert_norm_scale.reshape(1, -1),
        group_router_columns.T,
        expert_router_columns.T,
        routes.T,
        input_channel_taps,
        input_map_taps,
        output_map_taps,
        by_block(step_logits),
        by_block(extra_log_decay),
        gated_norm_scale.reshape(1, -1),
        head_log_rate,
        head_direct_scale,
        expert_gate_weight[0],
        expert_up_weight[0],
        expert_down_weight[0],
        mixer_output_weight,
        mixer_input_channels,
        output_gate_logits,
        head_group_input_map,
        head_group_output_map,
    )


def solution(mesh):
    in_specs = (
        P("ep", "tp"),
        P("ep", "tp"),
        P("ep", None),
        P("ep", None),
        P(None, "tp"),
        P(),
        P(),
        P("tp", "ep"),
        P("tp"),
        P("tp", "ep"),
        P("tp"),
        P("tp"),
        P("tp", None),
        P("ep", None),
        P(),
        P(),
        P(),
        P("ep", None),
        P("ep", None, "tp"),
        P("ep", None, "tp"),
        P("ep", "tp", None),
    )
    out_specs = (P(("ep", "tp"), None), P("ep", "tp"))
    return jax.shard_map(
        per_device, mesh=mesh, in_specs=in_specs, out_specs=out_specs, check_vma=False
    )
```

time: 150 us -> 104 us (0.69)
  local copies, waits for them, and re-layouts: 21.2 us -> 3.83 us
  Pallas kernels: 81.8 us -> 97.7 us
  other arithmetic: 12.4 us -> 0 us
  matrix products: 12.3 us -> 0 us
  starting transfers between devices: 10.6 us -> 0 us
  waiting for transfers between devices: 7.8 us -> 0 us
    pallas_call x1, Pallas kernels: 81.8 us -> 97.7 us  [fused(): pl.pallas_call(kernel, out_shape=(jax.ShapeDtypeStruct((128, 2048), bf16)...]
    dot_general x6 -> x0, matrix products: 12.3 us -> none  [the longest x1 4.57 us: mixer_half(): jnp.einsum('bls,hbls,bshp->blhp', scores, weight, x_dt, precision=exact_p...]
    all_to_all x1 -> x0, waiting for transfers between devices: 7.8 us -> none  [from_everyone(): lax.all_to_all(jnp.broadcast_to(value[None], (size, *value.shape)), axis,...]
    all_to_all x1 -> x0, starting transfers between devices: 6.53 us -> none  [from_everyone(): lax.all_to_all(jnp.broadcast_to(value[None], (size, *value.shape)), axis,...]
    convert_element_type x7 -> x0, other arithmetic: 6.25 us -> none  [the longest x1 2.6 us: mixer_half(): (gated.reshape(length, width) * gated_norm_scale.astype(jnp.float32)).ast...]
    reshape x5 -> x0, local copies, waits for them, and re-layouts: 5.82 us -> none  [the longest x2 5.61 us: mixer_half(): ssm = (inner + carried).reshape(length, heads_dev, head_dim)]
    ppermute x1 -> x0, starting transfers between devices: 4.05 us -> none  [from_behind(): lax.ppermute(value, axis, [(source, source + steps) for source in range(f...]
    mul x6 -> x0, local copies, waits for them, and re-layouts: 2.89 us -> none  [the longest x2 1.4 us: mixer_half(): gated * lax.rsqrt(jnp.mean(gated * gated, axis=-1, keepdims=True) + eps)]
  transfers between devices with their start and end apart: 2 -> 0, of which waited for: 1 -> 0; matrix products, arithmetic and copies ran while one was open for 5% -> 0% of each run, Pallas kernels for 0% -> 0%
where the time goes in v2:
time: 104 us; the launch traced here: 102 us
  Pallas kernels  97.7 us (94%)
  local copies, waits for them, and re-layouts  3.83 us (4%)
    pallas_call x1, Pallas kernels, fused(): pl.pallas_call(kernel, out_shape=(jax.ShapeDtypeStruct((128, 2048), bf16)...  97.7 us
    unnamed x6, local copies, waits for them, and re-layouts  3.23 us

profile of v2, /device:TPU:1, one launch (start us, length us, event | category | flops | bytes accessed | tf_op | source)
XLA Modules:
  0.0 102.2 jit_solution(10158485528392748613)
XLA Ops:
  0.6 0.0 copy-start.1
  0.6 0.7 copy-done.1
  1.3 0.6 reshape.22.nsc
  1.9 97.7 %shard_map.212 = (bf16[128,2048]{1,0:T(8,128)(2,1)}, bf16[256,128]{1,0:T(8,128)(2,1)}) custom-call(bf16[256,2048]{1,0:T(8,128)(2,1)} %tok.1, bf16[1,2048]{1,0:T(2,128)(2,1)} %reshape.22.nsc, bf16[4,2048]{1,0:T(4,128)(2,1)} %bitcast.21, bf16[16,2048]{1,0:T(8,128)(2,1)} %bitcast.20, s32[2,256]{1,0:T(2,128)} %bitcast.24, bf16[4,128]{1,0:T(4,128)(2,1)} %ut.1, ...), custom_call_target="tpu_custom_call" | custom-call | tf_op jit(solution)/shard_map/pallas_call | solution.py:443
  99.6 0.0 copy-start
  99.6 1.9 %copy.27 = bf16[128,2048]{1,0:T(8,128)(2,1)} copy(bf16[128,2048]{1,0:T(8,128)(2,1)} %get-tuple-element.4) | data formatting | bytes 1048576
  101.6 0.0 copy-done
  101.6 0.6 copy.28
Async XLA Ops:
  0.6 0.7 copy-start.1
  99.6 1.9 %copy-start = (bf16[256,128]{1,0:T(8,128)(2,1)S(1)}, bf16[256,128]{1,0:T(8,128)(2,1)}, u32[]{:S(2)}) copy-start(bf16[256,128]{1,0:T(8,128)(2,1)} %get-tuple-element.5) | copy-start | bytes 196612

commit v3 on v2

--- a/solution.py
+++ b/solution.py
@@ -14,14 +14,19 @@
 CAP = 64
 HALF = CAP // 2
 ORDER = (4, 3, 5, 2, 6, 1, 7, 0)
+NEAR = (
+    (0, 0), (1, 0), (0, 1), (3, 0), (0, 3), (1, 1), (3, 3), (1, 3),
+    (3, 1), (2, 0), (0, 2), (2, 1), (1, 2), (3, 2), (2, 3), (2, 2),
+)
+EARLY = 12
 
 
 def kernel(
-    tok, nsc, rg, re, rt, ut, bt, ct, sl, ex, gn, rate, direct,
-    gate_h, up_h, down_h, w_h, u_h, og_h, bm_h, cm_h,
+    nsc, rg, re, rt, ut, bt, ct, sl, ex, gn, rate, direct,
+    tok_h, gate_h, up_h, down_h, w_h, u_h, og_h, bm_h, cm_h,
     mo, eo,
     nrm, sbuf, xr, gw, uw, dn, hall, ysend, ybuf, zsend, zbuf, wg, mx, psend, precv,
-    ub, bb, cb, ogb, xsb, csb, c0l, c1l, dtl, cumr, dtr, tst, ssm, spad, ssend, sst, entb, mixb,
+    ub, bb, cb, ogb, xsb, csb, c0l, c1l, dtl, cumr, dtr, tst, ssm, spad, ssend, sst, entb, mixb, keep_mine, tok,
     loc_s, dnl_s, dns_s, dnr_s, xs_s, xr_s, xf_s, xg_s, hs_s, hr_s, ys_s, yr_s, zs_s, zr_s,
     ws_s, wr_s, ms_s, mr_s, fs_s, fr_s, hl_s, hh_s, ss_s, sr_s,
 ):
@@ -31,7 +36,8 @@
     other = z * 2 + (1 - c)
 
     def ep_at(d, sign):
-        return ((y + 4 + sign * (d // 4)) % 4) * 4 + (x + 4 + sign * (d % 4)) % 4
+        dx, dy = NEAR[d]
+        return ((y + 4 + sign * dy) % 4) * 4 + (x + 4 + sign * dx) % 4
 
     def tp_at(r):
         return ((z + r) % NZ) * 2 + c
@@ -49,6 +55,14 @@
             barrier, inc=1, device_id={"ep": e, "tp": t}, device_id_type=pl.DeviceIdType.MESH
         )
 
+    for d in range(1, NEP):
+        greet(ep_at(d, 1), tp)
+    for r in range(1, NZ):
+        greet(ep, tp_at(r))
+    greet(ep, other)
+
+    lt = pltpu.make_async_copy(tok_h, tok, loc_s.at[7])
+    lt.start()
     lg = pltpu.make_async_copy(gate_h, gw, loc_s.at[0])
     lu = pltpu.make_async_copy(up_h, uw, loc_s.at[1])
     lw = pltpu.make_async_copy(w_h, wg.at[pl.ds(0, 128), :], loc_s.at[2])
@@ -76,15 +90,13 @@
     for cp in dn_l:
         cp.start()
 
-    for d in range(1, NEP):
-        greet(ep_at(d, 1), tp)
-    for r in range(1, NZ):
-        greet(ep, tp_at(r))
-    greet(ep, other)
+    norm_gain = jnp.concatenate([nsc[i : i + 1, :] for i in range(16)], axis=1).astype(f32)
+    lt.wait()
+
     def norm_rows(i, _):
         rows = pl.ds(pl.multiple_of(i * 32, 32), 32)
         v = tok[rows, :].astype(f32)
-        v = v * lax.rsqrt(jnp.mean(v * v, axis=1, keepdims=True) + eps) * nsc[...].astype(f32)
+        v = v * lax.rsqrt(jnp.mean(v * v, axis=1, keepdims=True) + eps) * norm_gain
         nrm[rows, :] = v.astype(bf16)
         return 0
 
@@ -92,7 +104,9 @@
 
     r0, r1 = rt[0:1, :], rt[1:2, :]
     di = lax.broadcasted_iota(jnp.int32, (NEP, 256), 0)
-    e_rel = (((y + lax.shift_right_logical(di, 2)) & 3) * 4) + ((x + di) & 3)
+    e_rel = jnp.zeros((NEP, 256), jnp.int32)
+    for d in range(NEP):
+        e_rel = jnp.where(di == d, ep_at(d, 1), e_rel)
     in0, in1 = e_rel == r0, e_rel == r1
     routed = in0 | in1
     onehot = jnp.where(routed, 1.0, 0.0).astype(bf16)
@@ -125,26 +139,33 @@
     ]
     for cp in dn_r:
         cp.start()
-    def w_copy(way, k):
+    def w_copy(way, k, part):
         if way == 0:
             a, b, t = (9 - k) % NZ, NZ - k, tp_at(1)
         else:
             a, b, t = k - 1, k, tp_at(NZ - 1)
-        lo, n = (0, 128) if k < 4 else (64 * way, 64)
-        src = w_h.at[pl.ds(lo, n), :] if k == 1 else wg.at[pl.ds(a * 128 + lo, n), :]
+        lo = 64 * part
+        src = w_h.at[pl.ds(lo, 64), :] if k == 1 else wg.at[pl.ds(a * 128 + lo, 64), :]
         return push(
-            src, wg.at[pl.ds(b * 128 + lo, n), :], ws_s.at[way, k - 1], wr_s.at[way, k - 1], ep, t
+            src, wg.at[pl.ds(b * 128 + lo, 64), :],
+            ws_s.at[way, part, k - 1], wr_s.at[way, part, k - 1], ep, t,
         )
 
-    w_cp = [[w_copy(way, k) for k in range(1, 5)] for way in range(2)]
-
-    def w_step(k):
+    w_cp = {
+        (way, k, part): w_copy(way, k, part)
+        for way in range(2) for k in range(1, 5) for part in range(2)
+        if k < 4 or part == way
+    }
+
+    def w_step(k, part):
         for way in range(2):
-            if k > 1:
-                w_cp[way][k - 2].wait_recv()
-            w_cp[way][k - 1].start()
-
-    w_step(1)
+            if (way, k, part) in w_cp:
+                if k > 1:
+                    w_cp[way, k - 1, part].wait_recv()
+                w_cp[way, k, part].start()
+
+    w_step(1, 0)
+    w_step(1, 1)
 
     x_cp = [
         push(
@@ -154,7 +175,7 @@
         )
         for d in range(1, NEP)
     ]
-    for cp in x_cp[:7]:
+    for cp in x_cp[:EARLY]:
         cp.start()
     xr[pl.ds(pl.multiple_of(HALF * c, HALF), HALF), :] = sbuf[0:HALF, :]
 
@@ -257,9 +278,11 @@
         gained = lax.dot_general(bs, weighed, (((0,), (0,)), ((), ())), preferred_element_type=f32)
         return state * jnp.exp(last) + gained, since + last
 
-    state, since = lax.fori_loop(
-        0, 16, one_block, (jnp.zeros((128, 128), f32), jnp.zeros((1, 128), f32))
+    carry = lax.fori_loop(
+        0, 8, one_block, (jnp.zeros((128, 128), f32), jnp.zeros((1, 128), f32))
     )
+    w_step(2, 0)
+    state, since = lax.fori_loop(8, 16, one_block, carry)
     spad[...] = state
     half_rows = pl.ds(pl.multiple_of((grp % 2) * 64, 64), 64)
     ssend[0:64, :] = spad[half_rows, :].astype(bf16)
@@ -275,9 +298,9 @@
     ]
     for cp in s_cp:
         cp.start()
-    for cp in x_cp[7:]:
-        cp.start()
-    w_step(2)
+    for cp in x_cp[EARLY:]:
+        cp.start()
+    w_step(2, 1)
 
 
     def mixer_rest():
@@ -374,8 +397,11 @@
         if g == 0:
             for cq in dn_r:
                 cq.wait_recv()
+        if g == 0:
+            w_step(3, 0)
         if g == 2:
-            w_step(3)
+            w_step(4, 0)
+            w_step(4, 1)
             mixer_rest()
         cp.wait_recv()
         yv = jnp.dot(hall[0, rows, :], dn[0], preferred_element_type=f32)
@@ -384,9 +410,27 @@
         for d in range(4 * g, 4 * g + 4):
             if d > 0:
                 y_cp[0][d - 1].start()
+        if g == 1:
+            w_step(3, 1)
     for d in range(1, NEP):
         y_cp[1][d - 1].start()
     ybuf[0:CAP, :] = ysend[0:CAP, :]
+
+    def project():
+        lw.wait()
+        for cp in m_cp:
+            cp.wait_recv()
+        for way in range(2):
+            w_cp[way, 3, 1 - way].wait_recv()
+            w_cp[way, 4, way].wait_recv()
+        theirs = mx[pl.ds(pl.multiple_of((1 - c) * 128, 128), 128), :]
+        psend[...] = jnp.dot(theirs, wg[...], preferred_element_type=f32).astype(bf16)
+        fin = push(psend, precv, fs_s, fr_s, ep, other)
+        fin.start()
+        ours = mx[pl.ds(pl.multiple_of(c * 128, 128), 128), :]
+        mine = jnp.dot(ours, wg[...], preferred_element_type=f32)
+        keep_mine[...] = mine
+        return fin
 
     z_cp = []
     for h in range(2):
@@ -405,21 +449,10 @@
             cp.start()
             z_cp.append(cp)
         if h == 0:
-            w_step(4)
-
-    lw.wait()
-    for cp in m_cp:
-        cp.wait_recv()
-    for way in range(2):
-        w_cp[way][3].wait_recv()
-    theirs = mx[pl.ds(pl.multiple_of((1 - c) * 128, 128), 128), :]
-    psend[...] = jnp.dot(theirs, wg[...], preferred_element_type=f32).astype(bf16)
-    fin = push(psend, precv, fs_s, fr_s, ep, other)
-    fin.start()
-    ours = mx[pl.ds(pl.multiple_of(c * 128, 128), 128), :]
-    mine = jnp.dot(ours, wg[...], preferred_element_type=f32)
+            fin = project()
+
     fin.wait_recv()
-    mo[...] = (mine + precv[...].astype(f32)).astype(bf16)
+    mo[...] = (keep_mine[...] + precv[...].astype(f32)).astype(bf16)
 
     acc = zbuf[0].astype(f32)
     for cp in z_cp:
@@ -430,9 +463,8 @@
 
     for cp in dn_r + m_cp + x_cp + halo + s_cp + hand + y_cp[0] + y_cp[1] + h_cp + z_cp + [fin]:
         cp.wait_send()
-    for way in range(2):
-        for cp in w_cp[way]:
-            cp.wait_send()
+    for cp in w_cp.values():
+        cp.wait_send()
 
 
 def fused(*args):
@@ -443,10 +475,10 @@
     return pl.pallas_call(
         kernel,
         out_shape=(
-            jax.ShapeDtypeStruct((128, 2048), bf16),
-            jax.ShapeDtypeStruct((256, 128), bf16),
+            pltpu.VMEM((128, 2048), bf16),
+            pltpu.VMEM((256, 128), bf16),
         ),
-        in_specs=[vmem] * 11 + [smem] * 2 + [hbm] * 8,
+        in_specs=[vmem] * 10 + [smem] * 2 + [hbm] * 9,
         out_specs=(vmem, vmem),
         scratch_shapes=[
             v((256, 2048), bf16),
@@ -482,10 +514,12 @@
             v((16, 72, 128), bf16),
             v((128, 128), bf16),
             v((2048, 128), bf16),
-            dma((7,)), dma((8,)), dma((8,)), dma((8,)),
+            v((128, 2048), f32),
+            v((256, 2048), bf16),
+            dma((8,)), dma((8,)), dma((8,)), dma((8,)),
             dma((16,)), dma((16,)), dma((16,)), dma((16,)),
             dma((4,)), dma((4,)), dma((2, 16)), dma((2, 16)),
-            dma((8,)), dma((8,)), dma((2, 4)), dma((2, 4)), dma((8,)), dma((8,)),
+            dma((8,)), dma((8,)), dma((2, 2, 4)), dma((2, 2, 4)), dma((8,)), dma((8,)),
             dma, dma, dma((3,)), dma((3,)), dma((16,)), dma((16,)),
         ],
         compiler_params=pltpu.CompilerParams(
@@ -521,8 +555,7 @@
         return jnp.transpose(v.reshape(2, 16, 128), (1, 0, 2)).reshape(32, 128)
 
     return fused(
-        second_batch_tokens,
-        pre_expert_norm_scale.reshape(1, -1),
+        pre_expert_norm_scale.reshape(16, 128),
         group_router_columns.T,
         expert_router_columns.T,
         routes.T,
@@ -534,6 +567,7 @@
         gated_norm_scale.reshape(1, -1),
         head_log_rate,
         head_direct_scale,
+        second_batch_tokens,
         expert_gate_weight[0],
         expert_up_weight[0],
         expert_down_weight[0],

time: 104 us -> 82.4 us (0.79)
  the two profiles are of different devices: /device:TPU:1 before, /device:TPU:32 now
where the time goes in v3:
time: 82.4 us; the launch traced here: 82.3 us
  Pallas kernels  80.2 us (97%)
  local copies, waits for them, and re-layouts  1.42 us (2%)
    pallas_call x1, Pallas kernels, fused(): pl.pallas_call(kernel, out_shape=(pltpu.VMEM((128, 2048), bf16), pltpu.VM...  80.2 us

profile of v3, /device:TPU:32, one launch (start us, length us, event | category | flops | bytes accessed | tf_op | source)
XLA Modules:
  0.0 82.3 jit_solution(3225882161046862517)
XLA Ops:
  0.6 80.2 %shard_map.212 = (bf16[128,2048]{1,0:T(8,128)(2,1)S(1)}, bf16[256,128]{1,0:T(8,128)(2,1)S(1)}) custom-call(bf16[16,128]{1,0:T(8,128)(2,1)} %bitcast.25, bf16[4,2048]{1,0:T(4,128)(2,1)} %bitcast.22, bf16[16,2048]{1,0:T(8,128)(2,1)} %bitcast.21, s32[2,256]{1,0:T(2,128)} %bitcast.26, bf16[4,128]{1,0:T(4,128)(2,1)} %ut.1, bf16[4,256]{1,0:T(4,128)(2,1)} %bt.1, ...), custom_call_target="tpu_custom_call" | custom-call | tf_op jit(solution)/shard_map/pallas_call | solution.py:475
  80.9 0.8 copy.27
  81.7 0.6 copy.28

commit v4 on v3

--- a/solution.py
+++ b/solution.py
@@ -13,22 +13,23 @@
 NZ = 8
 CAP = 64
 HALF = CAP // 2
-ORDER = (4, 3, 5, 2, 6, 1, 7, 0)
+ORDER = (4, 3, 5, 1, 2, 6, 7, 0)
 NEAR = (
     (0, 0), (1, 0), (0, 1), (3, 0), (0, 3), (1, 1), (3, 3), (1, 3),
     (3, 1), (2, 0), (0, 2), (2, 1), (1, 2), (3, 2), (2, 3), (2, 2),
 )
-EARLY = 12
+EARLY = 16
 
 
 def kernel(
-    nsc, rg, re, rt, ut, bt, ct, sl, ex, gn, rate, direct,
+    nsc_h, rg_h, re_h, rt_h, ut_h, bt_h, ct_h, sl_h, ex_h, gn_h, rate, direct,
     tok_h, gate_h, up_h, down_h, w_h, u_h, og_h, bm_h, cm_h,
     mo, eo,
     nrm, sbuf, xr, gw, uw, dn, hall, ysend, ybuf, zsend, zbuf, wg, mx, psend, precv,
-    ub, bb, cb, ogb, xsb, csb, c0l, c1l, dtl, cumr, dtr, tst, ssm, spad, ssend, sst, entb, mixb, keep_mine, tok,
+    ub, bb, cb, ogb, xsb, csb, c0l, c1l, dtl, cumr, dtr, tst, ssm, spad, ssend, sst, entb, mixb, keep_mine, tok, zway, zown,
+    nsc, rg, re, rt, ut, bt, ct, sl, ex, gn, small_s,
     loc_s, dnl_s, dns_s, dnr_s, xs_s, xr_s, xf_s, xg_s, hs_s, hr_s, ys_s, yr_s, zs_s, zr_s,
-    ws_s, wr_s, ms_s, mr_s, fs_s, fr_s, hl_s, hh_s, ss_s, sr_s,
+    ws_s, wr_s, ms_s, mr_s, fs_s, fr_s, hl_s, hh_s, ss_s, sr_s, zws_s, zwr_s,
 ):
     ep, tp = lax.axis_index("ep"), lax.axis_index("tp")
     y, x = ep // 4, ep % 4
@@ -61,8 +62,19 @@
         greet(ep, tp_at(r))
     greet(ep, other)
 
+    small = [
+        pltpu.make_async_copy(src, dst, small_s.at[i])
+        for i, (src, dst) in enumerate((
+            (rt_h, rt), (nsc_h, nsc), (rg_h, rg), (re_h, re), (ut_h, ut), (bt_h, bt),
+            (ct_h, ct), (sl_h, sl), (ex_h, ex), (gn_h, gn),
+        ))
+    ]
+    for cp in small[:2]:
+        cp.start()
     lt = pltpu.make_async_copy(tok_h, tok, loc_s.at[7])
     lt.start()
+    for cp in small[2:]:
+        cp.start()
     lg = pltpu.make_async_copy(gate_h, gw, loc_s.at[0])
     lu = pltpu.make_async_copy(up_h, uw, loc_s.at[1])
     lw = pltpu.make_async_copy(w_h, wg.at[pl.ds(0, 128), :], loc_s.at[2])
@@ -90,6 +102,8 @@
     for cp in dn_l:
         cp.start()
 
+    for cp in small:
+        cp.wait()
     norm_gain = jnp.concatenate([nsc[i : i + 1, :] for i in range(16)], axis=1).astype(f32)
     lt.wait()
 
@@ -179,6 +193,18 @@
         cp.start()
     xr[pl.ds(pl.multiple_of(HALF * c, HALF), HALF), :] = sbuf[0:HALF, :]
 
+    def x_hand(d):
+        rows = pl.ds(pl.multiple_of(d * CAP + HALF * c, HALF), HALF)
+        return push(xr.at[rows, :], xr.at[rows, :], xf_s.at[d], xg_s.at[d], ep, other)
+
+    hand = [x_hand(d) for d in range(NEP)]
+
+    def pass_on(g):
+        for d in range(4 * g, 4 * g + 4):
+            if d > 0:
+                x_cp[d - 1].wait_recv()
+            hand[d].start()
+
     nt = (((1,), (1,)), ((), ()))
     gl = lax.dot_general(rg[...], tokens_n, nt, preferred_element_type=f32)
     el = lax.dot_general(re[...], tokens_n, nt, preferred_element_type=f32)
@@ -366,12 +392,6 @@
     for cp in dn_l:
         cp.wait()
 
-    def x_hand(d):
-        rows = pl.ds(pl.multiple_of(d * CAP + HALF * c, HALF), HALF)
-        return push(xr.at[rows, :], xr.at[rows, :], xf_s.at[d], xg_s.at[d], ep, other)
-
-    hand = [x_hand(d) for d in range(NEP)]
-
     def y_copy(d, h):
         part = (pl.ds(d * CAP, CAP), pl.ds(h * 512, 512))
         return push(ysend.at[part], ybuf.at[part], ys_s.at[h, d], yr_s.at[h, d], ep_at(d, -1), tp)
@@ -379,10 +399,10 @@
     y_cp = [[y_copy(d, h) for d in range(1, NEP)] for h in range(2)]
     h_cp = []
     for g in range(4):
-        for d in range(4 * g, 4 * g + 4):
-            if d > 0:
-                x_cp[d - 1].wait_recv()
-            hand[d].start()
+        part = hall.at[c, pl.ds(256 * g, 256), :]
+        h_cp.append(push(part, part, hs_s.at[g], hr_s.at[g], ep, other))
+
+    def hidden(g):
         for d in range(4 * g, 4 * g + 4):
             hand[d].wait_recv()
         rows = slice(256 * g, 256 * (g + 1))
@@ -390,30 +410,39 @@
         gv = jnp.dot(xg, gw[...], preferred_element_type=f32)
         uv = jnp.dot(xg, uw[...], preferred_element_type=f32)
         hall[c, rows, :] = (gv * jax.nn.sigmoid(gv) * uv).astype(bf16)
-        part = hall.at[c, pl.ds(256 * g, 256), :]
-        cp = push(part, part, hs_s.at[g], hr_s.at[g], ep, other)
-        cp.start()
-        h_cp.append(cp)
-        if g == 0:
-            for cq in dn_r:
-                cq.wait_recv()
-        if g == 0:
-            w_step(3, 0)
-        if g == 2:
-            w_step(4, 0)
-            w_step(4, 1)
-            mixer_rest()
-        cp.wait_recv()
+        h_cp[g].start()
+
+    def results(g):
+        rows = slice(256 * g, 256 * (g + 1))
+        h_cp[g].wait_recv()
         yv = jnp.dot(hall[0, rows, :], dn[0], preferred_element_type=f32)
         yv += jnp.dot(hall[1, rows, :], dn[1], preferred_element_type=f32)
         ysend[rows, :] = yv.astype(bf16)
         for d in range(4 * g, 4 * g + 4):
             if d > 0:
                 y_cp[0][d - 1].start()
-        if g == 1:
-            w_step(3, 1)
+
+    pass_on(0)
+    pass_on(1)
+    hidden(0)
+    hidden(1)
+    for cq in dn_r:
+        cq.wait_recv()
+    w_step(3, 0)
+    results(0)
+    results(1)
+    w_step(3, 1)
+    pass_on(2)
+    hidden(2)
+    pass_on(3)
+    results(2)
+    hidden(3)
+    results(3)
     for d in range(1, NEP):
         y_cp[1][d - 1].start()
+    w_step(4, 0)
+    w_step(4, 1)
+    mixer_rest()
     ybuf[0:CAP, :] = ysend[0:CAP, :]
 
     def project():
@@ -432,36 +461,50 @@
         keep_mine[...] = mine
         return fin
 
-    z_cp = []
+    first_hop = {4: (2, 0), 3: (1, 1), 5: (7, 2)}
+    z_cp, on_way = [], []
     for h in range(2):
         for d in range(1, NEP):
             y_cp[h][d - 1].wait_recv()
         cols = slice(512 * h, 512 * (h + 1))
         comb = jnp.dot(mixw, ybuf[:, cols], preferred_element_type=f32)
-        for i in range(4):
+        for i in ((0, 1, 2, 3), (2, 3, 0, 1))[h]:
             r = ORDER[4 * h + i]
+            if r == 2:
+                for cp in on_way:
+                    cp.wait_recv()
             val = comb[:, 128 * i : 128 * (i + 1)]
             if r == 0:
-                zbuf[0] = val.astype(bf16)
+                zown[...] = val
                 continue
+            if r in first_hop:
+                hop, place_w = first_hop[r]
+                zsend[r] = val.astype(bf16)
+                cp = push(zsend.at[r], zway.at[place_w], zws_s.at[place_w], zwr_s.at[place_w], ep, tp_at(hop))
+                cp.start()
+                on_way.append(cp)
+                continue
+            if r == 2:
+                val = val + zway[0].astype(f32) + zway[1].astype(f32)
+            if r == 6:
+                val = val + zway[2].astype(f32)
             zsend[r] = val.astype(bf16)
             cp = push(zsend.at[r], zbuf.at[NZ - r], zs_s.at[NZ - r], zr_s.at[NZ - r], ep, tp_at(r))
             cp.start()
             z_cp.append(cp)
-        if h == 0:
-            fin = project()
-
+
+    fin = project()
     fin.wait_recv()
     mo[...] = (keep_mine[...] + precv[...].astype(f32)).astype(bf16)
 
-    acc = zbuf[0].astype(f32)
+    acc = zown[...]
     for cp in z_cp:
         cp.wait_recv()
-    for r in range(1, NZ):
+    for r in (1, 2, 6, 7):
         acc += zbuf[r].astype(f32)
     eo[...] = acc.astype(bf16)
 
-    for cp in dn_r + m_cp + x_cp + halo + s_cp + hand + y_cp[0] + y_cp[1] + h_cp + z_cp + [fin]:
+    for cp in dn_r + m_cp + x_cp + halo + s_cp + hand + y_cp[0] + y_cp[1] + h_cp + z_cp + on_way + [fin]:
         cp.wait_send()
     for cp in w_cp.values():
         cp.wait_send()
@@ -478,7 +521,7 @@
             pltpu.VMEM((128, 2048), bf16),
             pltpu.VMEM((256, 128), bf16),
         ),
-        in_specs=[vmem] * 10 + [smem] * 2 + [hbm] * 9,
+        in_specs=[hbm] * 10 + [smem] * 2 + [hbm] * 9,
         out_specs=(vmem, vmem),
         scratch_shapes=[
             v((256, 2048), bf16),
@@ -516,11 +559,25 @@
             v((2048, 128), bf16),
             v((128, 2048), f32),
             v((256, 2048), bf16),
+            v((3, 256, 128), bf16),
+            v((256, 128), f32),
+            v((16, 128), bf16),
+            v((4, 2048), bf16),
+            v((16, 2048), bf16),
+            v((2, 256), jnp.int32),
+            v((4, 128), bf16),
+            v((4, 256), bf16),
+            v((4, 256), bf16),
+            v((32, 128), f32),
+            v((32, 128), f32),
+            v((1, 128), bf16),
+            dma((10,)),
             dma((8,)), dma((8,)), dma((8,)), dma((8,)),
             dma((16,)), dma((16,)), dma((16,)), dma((16,)),
             dma((4,)), dma((4,)), dma((2, 16)), dma((2, 16)),
             dma((8,)), dma((8,)), dma((2, 2, 4)), dma((2, 2, 4)), dma((8,)), dma((8,)),
             dma, dma, dma((3,)), dma((3,)), dma((16,)), dma((16,)),
+            dma((3,)), dma((3,)),
         ],
         compiler_params=pltpu.CompilerParams(
             collective_id=0, has_side_effects=True, vmem_limit_bytes=56 * 1024 * 1024

time: 82.4 us -> 78.3 us (0.950)
  the two profiles are of different devices: /device:TPU:32 before, /device:TPU:1 now
where the time goes in v4:
time: 78.3 us; the launch traced here: 77.9 us
  Pallas kernels  75.8 us (97%)
  local copies, waits for them, and re-layouts  1.42 us (2%)
    pallas_call x1, Pallas kernels, fused(): pl.pallas_call(kernel, out_shape=(pltpu.VMEM((128, 2048), bf16), pltpu.VM...  75.8 us

profile of v4, /device:TPU:1, one launch (start us, length us, event | category | flops | bytes accessed | tf_op | source)
XLA Modules:
  0.0 77.9 jit_solution(10865350488180250548)
XLA Ops:
  0.6 75.8 %shard_map.212 = (bf16[128,2048]{1,0:T(8,128)(2,1)S(1)}, bf16[256,128]{1,0:T(8,128)(2,1)S(1)}) custom-call(bf16[16,128]{1,0:T(8,128)(2,1)} %bitcast.25, bf16[4,2048]{1,0:T(4,128)(2,1)} %bitcast.22, bf16[16,2048]{1,0:T(8,128)(2,1)} %bitcast.21, s32[2,256]{1,0:T(2,128)} %bitcast.26, bf16[4,128]{1,0:T(4,128)(2,1)} %ut_h.1, bf16[4,256]{1,0:T(4,128)(2,1)} %bt_h.1, ...), custom_call_target="tpu_custom_call" | custom-call | tf_op jit(solution)/shard_map/pallas_call | solution.py:518
  76.4 0.8 %copy.27 = bf16[128,2048]{1,0:T(8,128)(2,1)} copy(bf16[128,2048]{1,0:T(8,128)(2,1)S(1)} %get-tuple-element.2) | data formatting | bytes 1048576
  77.2 0.6 copy.28

commit v5 on v4

--- a/solution.py
+++ b/solution.py
@@ -27,7 +27,7 @@
     mo, eo,
     nrm, sbuf, xr, gw, uw, dn, hall, ysend, ybuf, zsend, zbuf, wg, mx, psend, precv,
     ub, bb, cb, ogb, xsb, csb, c0l, c1l, dtl, cumr, dtr, tst, ssm, spad, ssend, sst, entb, mixb, keep_mine, tok, zway, zown,
-    nsc, rg, re, rt, ut, bt, ct, sl, ex, gn, small_s,
+    nsc, rg, re, rt, ut, bt, ct, sl, ex, gn, small_s, tok_s,
     loc_s, dnl_s, dns_s, dnr_s, xs_s, xr_s, xf_s, xg_s, hs_s, hr_s, ys_s, yr_s, zs_s, zr_s,
     ws_s, wr_s, ms_s, mr_s, fs_s, fr_s, hl_s, hh_s, ss_s, sr_s, zws_s, zwr_s,
 ):
@@ -56,6 +56,12 @@
             barrier, inc=1, device_id={"ep": e, "tp": t}, device_id_type=pl.DeviceIdType.MESH
         )
 
+    lt = [
+        pltpu.make_async_copy(tok_h.at[pl.ds(64 * i, 64), :], tok.at[pl.ds(64 * i, 64), :], tok_s.at[i])
+        for i in range(4)
+    ]
+    for cp in lt:
+        cp.start()
     for d in range(1, NEP):
         greet(ep_at(d, 1), tp)
     for r in range(1, NZ):
@@ -69,11 +75,7 @@
             (ct_h, ct), (sl_h, sl), (ex_h, ex), (gn_h, gn),
         ))
     ]
-    for cp in small[:2]:
-        cp.start()
-    lt = pltpu.make_async_copy(tok_h, tok, loc_s.at[7])
-    lt.start()
-    for cp in small[2:]:
+    for cp in small:
         cp.start()
     lg = pltpu.make_async_copy(gate_h, gw, loc_s.at[0])
     lu = pltpu.make_async_copy(up_h, uw, loc_s.at[1])
@@ -87,7 +89,7 @@
         pltpu.make_async_copy(cm_h.at[:, map_cols], cb.at[body, :], loc_s.at[6]),
         pltpu.make_async_copy(og_h, ogb, loc_s.at[3]),
     ]
-    for cp in l_mix + [lg, lu, lw]:
+    for cp in l_mix + [lw]:
         cp.start()
 
     def down_cols(q, core):
@@ -99,13 +101,10 @@
         )
         for q in range(NZ)
     ]
-    for cp in dn_l:
-        cp.start()
 
     for cp in small:
         cp.wait()
     norm_gain = jnp.concatenate([nsc[i : i + 1, :] for i in range(16)], axis=1).astype(f32)
-    lt.wait()
 
     def norm_rows(i, _):
         rows = pl.ds(pl.multiple_of(i * 32, 32), 32)
@@ -114,7 +113,9 @@
         nrm[rows, :] = v.astype(bf16)
         return 0
 
-    lax.fori_loop(0, 8, norm_rows, 0)
+    for i in range(4):
+        lt[i].wait()
+        lax.fori_loop(2 * i, 2 * i + 2, norm_rows, 0)
 
     r0, r1 = rt[0:1, :], rt[1:2, :]
     di = lax.broadcasted_iota(jnp.int32, (NEP, 256), 0)
@@ -190,6 +191,8 @@
         for d in range(1, NEP)
     ]
     for cp in x_cp[:EARLY]:
+        cp.start()
+    for cp in dn_l + [lg, lu]:
         cp.start()
     xr[pl.ds(pl.multiple_of(HALF * c, HALF), HALF), :] = sbuf[0:HALF, :]
 
@@ -572,6 +575,7 @@
             v((32, 128), f32),
             v((1, 128), bf16),
             dma((10,)),
+            dma((4,)),
             dma((8,)), dma((8,)), dma((8,)), dma((8,)),
             dma((16,)), dma((16,)), dma((16,)), dma((16,)),
             dma((4,)), dma((4,)), dma((2, 16)), dma((2, 16)),

time: 78.3 us -> 77.5 us (0.990)
  no operation moved by 1% of the time
where the time goes in v5:
time: 77.5 us; the launch traced here: 77.4 us
  Pallas kernels  75.3 us (97%)
  local copies, waits for them, and re-layouts  1.42 us (2%)
    pallas_call x1, Pallas kernels, fused(): pl.pallas_call(kernel, out_shape=(pltpu.VMEM((128, 2048), bf16), pltpu.VM...  75.3 us

profile of v5, /device:TPU:1, one launch (start us, length us, event | category | flops | bytes accessed | tf_op | source)
XLA Modules:
  0.0 77.4 jit_solution(16534679940410942863)
XLA Ops:
  0.6 75.3 %shard_map.212 = (bf16[128,2048]{1,0:T(8,128)(2,1)S(1)}, bf16[256,128]{1,0:T(8,128)(2,1)S(1)}) custom-call(bf16[16,128]{1,0:T(8,128)(2,1)} %bitcast.25, bf16[4,2048]{1,0:T(4,128)(2,1)} %bitcast.22, bf16[16,2048]{1,0:T(8,128)(2,1)} %bitcast.21, s32[2,256]{1,0:T(2,128)} %bitcast.26, bf16[4,128]{1,0:T(4,128)(2,1)} %ut_h.1, bf16[4,256]{1,0:T(4,128)(2,1)} %bt_h.1, ...), custom_call_target="tpu_custom_call" | custom-call | tf_op jit(solution)/shard_map/pallas_call | solution.py:521
  75.9 0.8 %copy.27 = bf16[128,2048]{1,0:T(8,128)(2,1)} copy(bf16[128,2048]{1,0:T(8,128)(2,1)S(1)} %get-tuple-element.2) | data formatting | bytes 1048576
  76.7 0.6 copy.28

commit v6 on v5

--- a/solution.py
+++ b/solution.py
@@ -18,7 +18,6 @@
     (0, 0), (1, 0), (0, 1), (3, 0), (0, 3), (1, 1), (3, 3), (1, 3),
     (3, 1), (2, 0), (0, 2), (2, 1), (1, 2), (3, 2), (2, 3), (2, 2),
 )
-EARLY = 16
 
 
 def kernel(
@@ -107,7 +106,7 @@
     norm_gain = jnp.concatenate([nsc[i : i + 1, :] for i in range(16)], axis=1).astype(f32)
 
     def norm_rows(i, _):
-        rows = pl.ds(pl.multiple_of(i * 32, 32), 32)
+        rows = pl.ds(pl.multiple_of(i * 16, 16), 16)
         v = tok[rows, :].astype(f32)
         v = v * lax.rsqrt(jnp.mean(v * v, axis=1, keepdims=True) + eps) * norm_gain
         nrm[rows, :] = v.astype(bf16)
@@ -115,7 +114,7 @@
 
     for i in range(4):
         lt[i].wait()
-        lax.fori_loop(2 * i, 2 * i + 2, norm_rows, 0)
+        lax.fori_loop(4 * i, 4 * i + 4, norm_rows, 0)
 
     r0, r1 = rt[0:1, :], rt[1:2, :]
     di = lax.broadcasted_iota(jnp.int32, (NEP, 256), 0)
@@ -132,12 +131,6 @@
     place = jnp.where(routed, place, -1.0)
     slot = lax.broadcasted_iota(jnp.int32, (HALF, 256), 0) + HALF * c
     slot = slot.astype(f32)
-    tokens_n = nrm[...]
-    for q in range(4):
-        pick = jnp.concatenate(
-            [jnp.where(place[d : d + 1, :] == slot, 1.0, 0.0) for d in range(4 * q, 4 * q + 4)], axis=0
-        ).astype(bf16)
-        sbuf[q * 128 : (q + 1) * 128, :] = jnp.dot(pick, tokens_n, preferred_element_type=f32).astype(bf16)
     pl.semaphore_wait(barrier, NEP - 1 + NZ - 1 + 1)
     after = (ep + 1) % NEP
     halo = [
@@ -152,8 +145,6 @@
         push(down_cols(q, 1 - c), dn.at[c, :, pl.ds(q * 128, 128)], dns_s.at[q], dnr_s.at[q], ep, other)
         for q in range(NZ)
     ]
-    for cp in dn_r:
-        cp.start()
     def w_copy(way, k, part):
         if way == 0:
             a, b, t = (9 - k) % NZ, NZ - k, tp_at(1)
@@ -190,9 +181,15 @@
         )
         for d in range(1, NEP)
     ]
-    for cp in x_cp[:EARLY]:
-        cp.start()
-    for cp in dn_l + [lg, lu]:
+    tokens_n = nrm[...]
+    for q in range(4):
+        pick = jnp.concatenate(
+            [jnp.where(place[d : d + 1, :] == slot, 1.0, 0.0) for d in range(4 * q, 4 * q + 4)], axis=0
+        ).astype(bf16)
+        sbuf[q * 128 : (q + 1) * 128, :] = jnp.dot(pick, tokens_n, preferred_element_type=f32).astype(bf16)
+        for d in range(max(1, 4 * q), 4 * q + 4):
+            x_cp[d - 1].start()
+    for cp in dn_r + dn_l + [lg, lu]:
         cp.start()
     xr[pl.ds(pl.multiple_of(HALF * c, HALF), HALF), :] = sbuf[0:HALF, :]
 
@@ -327,8 +324,6 @@
     ]
     for cp in s_cp:
         cp.start()
-    for cp in x_cp[EARLY:]:
-        cp.start()
     w_step(2, 1)
 
 
@@ -474,6 +469,7 @@
         for i in ((0, 1, 2, 3), (2, 3, 0, 1))[h]:
             r = ORDER[4 * h + i]
             if r == 2:
+                fin = project()
                 for cp in on_way:
                     cp.wait_recv()
             val = comb[:, 128 * i : 128 * (i + 1)]
@@ -496,7 +492,6 @@
             cp.start()
             z_cp.append(cp)
 
-    fin = project()
     fin.wait_recv()
     mo[...] = (keep_mine[...] + precv[...].astype(f32)).astype(bf16)
 

time: 77.5 us -> 77.1 us (level)
  no operation moved by 1% of the time
where the time goes in v6:
time: 77.1 us; the launch traced here: 76.9 us
  Pallas kernels  74.8 us (97%)
  local copies, waits for them, and re-layouts  1.42 us (2%)
    pallas_call x1, Pallas kernels, fused(): pl.pallas_call(kernel, out_shape=(pltpu.VMEM((128, 2048), bf16), pltpu.VM...  74.8 us

profile of v6, /device:TPU:1, one launch (start us, length us, event | category | flops | bytes accessed | tf_op | source)
XLA Modules:
  0.0 76.9 jit_solution(4344124590248081378)
XLA Ops:
  0.6 74.8 %shard_map.212 = (bf16[128,2048]{1,0:T(8,128)(2,1)S(1)}, bf16[256,128]{1,0:T(8,128)(2,1)S(1)}) custom-call(bf16[16,128]{1,0:T(8,128)(2,1)} %bitcast.25, bf16[4,2048]{1,0:T(4,128)(2,1)} %bitcast.22, bf16[16,2048]{1,0:T(8,128)(2,1)} %bitcast.21, s32[2,256]{1,0:T(2,128)} %bitcast.26, bf16[4,128]{1,0:T(4,128)(2,1)} %ut_h.1, bf16[4,256]{1,0:T(4,128)(2,1)} %bt_h.1, ...), custom_call_target="tpu_custom_call" | custom-call | tf_op jit(solution)/shard_map/pallas_call | solution.py:516
  75.4 0.8 %copy.27 = bf16[128,2048]{1,0:T(8,128)(2,1)} copy(bf16[128,2048]{1,0:T(8,128)(2,1)S(1)} %get-tuple-element.2) | data formatting | bytes 1048576
  76.2 0.6 copy.28
